TPU v7x, 512 devices: a whole 4x4x16 slice. The times are simulated.
512 devices in a mesh: sp: 128 (over z, x, core), tp: 4 (over y).
Axes of the slice: x: 4, y: 4, z: 16, core: 2. Of those that a mesh axis runs over, the one named last changes fastest.
Arguments:
- queries: bfloat16 [32768, 1024], P('sp', 'tp'), may hold values from -6 to 6
- keys: bfloat16 [32768, 1024], P('sp', 'tp'), may hold values from -6 to 6
- values: bfloat16 [32768, 2048], P('sp', 'tp'), may hold values from -6 to 6
- gate_code: bfloat16 [32768, 32], P('sp'), may hold values from -5.5 to 5.5
- gate_up: bfloat16 [32, 1024], P(None, 'tp'), may hold values from -1 to 1
- gate_bias: float32 [1024], P('tp'), as said below
- gla_gain: float32 [256], replicated, may hold values from 0.1 to 1.9
- conv_input: bfloat16 [32768, 2048], P('sp', 'tp'), may hold values from -6 to 6
- conv_gate: bfloat16 [32768, 2048], P('sp', 'tp'), may hold values from -6 to 6
- conv_taps: float32 [3, 2048], P(None, 'tp'), may hold values from -3.5 to 3.5
- out_gla: bfloat16 [2048, 2048], P('tp', 'sp'), may hold values from -0.09375 to 0.09375
- out_conv: bfloat16 [2048, 2048], P('tp', 'sp'), may hold values from -0.09375 to 0.09375
Outputs:
- mixed: bfloat16 [32768, 2048], P(('sp', 'tp'))
Inputs may be any that keep to these rules, and one draw needn't show every extreme that they name: `gate_bias`: every bias is at least 1.5, so every decay per step lies strictly between 0 and 1.
All inputs are finite; a program needn't handle non-finite values.
Results may differ from a plain program's by a relative error of at most 0.028.
Values may be sent and summed in bfloat16 or wider, within the bound.
A program may use at most 64 MiB of HBM per device.

v0:
```python
import jax
import jax.numpy as jnp
from jax import lax
from jax.sharding import Mesh
from jax.sharding import PartitionSpec as P

KEY_WIDTH = 128
HEAD_V = 256
SEGMENT_LENGTH = 64
SP = ("sp_0", "sp_1", "sp_2")
SP_TP = ("sp_0", "sp_1", "sp_2", "tp")


softness_divisor = 16.0
epsilon = 1.0


def split_up(x, dim, count):
    dims = x.shape
    parts = x.reshape(*dims[:dim], count, dims[dim] // count, *dims[dim + 1 :])
    return jnp.moveaxis(parts, dim, 0)


def laid_out(parts, dim):
    parts = jnp.moveaxis(parts, 0, dim)
    dims = parts.shape
    return parts.reshape(*dims[:dim], dims[dim] * dims[dim + 1], *dims[dim + 2 :])


def turned_blocks(parts, axes, turns):
    inside = parts.shape[1:]
    out = parts.reshape(*(lax.axis_size(a) for a in axes), *inside)
    for k in turns:
        out = lax.all_to_all(out, axes[k], k, k, tiled=True)
    return out.reshape(-1, *inside)


def exchange_by_chip(x, groups, turns, split_dim, concat_dim):
    count = lax.axis_size(groups[0]) * lax.axis_size(groups[1])
    parts = split_up(x, split_dim, count)
    return laid_out(turned_blocks(parts, groups, turns), concat_dim)


def all_blocks(x, axes, turns):
    parts = x[None]
    for k in turns:
        parts = lax.all_gather(parts, axes[k], axis=0, tiled=True)
    current = [lax.axis_size(axes[k]) for k in reversed(turns)]
    parts = parts.reshape(*current, *x.shape)
    turned = sorted(range(len(turns)), key=lambda place: turns[len(turns) - 1 - place])
    return parts.transpose(*turned, *range(len(turns), parts.ndim)).reshape(-1, *x.shape)


def whole_of(x, axes, turns, dim):
    return laid_out(all_blocks(x, axes, turns), dim)


def for_sending(x):
    return jax.tree.map(lambda a: a.astype(jnp.bfloat16) if a.dtype == jnp.float32 else a, x)


def from_behind(x, axis, by):
    count = lax.axis_size(axis)
    pairs = [(i, i + by) for i in range(count) if 0 <= i + by < count]
    return lax.ppermute(x, axis, pairs)


def turned_gather(arrays, axis, dims):
    turned = [jnp.moveaxis(a, dim, 0) for a, dim in zip(arrays, dims)]
    both = jnp.concatenate([t.reshape(len(t), -1) for t in turned], axis=1)
    out, at, outs = (lax.all_gather(both, axis, axis=0, tiled=True), 0, [])
    for t, dim in zip(turned, dims):
        piece = out[:, at : at + t[0].size].reshape(-1, *t.shape[1:])
        outs.append(jnp.moveaxis(piece, 0, dim))
        at += t[0].size
    return tuple(outs)


def sent_and_summed(x, axis, dim):
    parts = split_up(x, dim, lax.axis_size(axis))
    arrived = lax.all_to_all(parts, axis, split_axis=0, concat_axis=0, tiled=True)
    return arrived.astype(jnp.float32).sum(axis=0)


def chain(earlier, latter):
    return (earlier[0] * latter[0], latter[0][..., None] * earlier[1] + latter[1])


def per_device(
    queries,
    keys,
    values,
    gate_code,
    gate_up,
    gate_bias,
    gla_gain,
    conv_input,
    conv_gate,
    conv_taps,
    out_gla,
    out_conv,
):
    row_count = queries.shape[0]
    segment_count = row_count // SEGMENT_LENGTH
    head_count = queries.shape[1] // KEY_WIDTH
    gate_score = jnp.dot(gate_code, gate_up, preferred_element_type=jnp.float32) + gate_bias
    decay_logarithm = (jax.nn.log_sigmoid(gate_score) / softness_divisor).reshape(
        segment_count, SEGMENT_LENGTH, head_count, KEY_WIDTH
    )
    inside = jnp.cumsum(decay_logarithm, axis=1)
    seg_total = inside[:, -1]
    key_blocks = keys.reshape(segment_count, SEGMENT_LENGTH, head_count, KEY_WIDTH)
    scaled_keys = (key_blocks * jnp.exp(seg_total[:, None] - inside)).astype(jnp.bfloat16)
    value_blocks = values.reshape(segment_count, SEGMENT_LENGTH, head_count, HEAD_V)
    update = jnp.einsum(
        "nshk,nshv->nhkv", scaled_keys, value_blocks, preferred_element_type=jnp.float32
    )
    through, local_state = lax.associative_scan(chain, (jnp.exp(seg_total), update), axis=0)
    device_decay = through[-1]
    device_state = local_state[-1]
    columns = exchange_by_chip(
        device_state[None].astype(jnp.bfloat16), (("sp_0", "sp_1"), "sp_2"), (1, 0), 3, 0
    ).astype(jnp.float32)
    decays = whole_of(device_decay[None], SP, (0, 1, 2), 0)
    running = lax.associative_scan(chain, (decays, columns), axis=0)[1]
    before = jnp.concatenate([jnp.zeros_like(running[:1]), running[:-1]], axis=0)
    incoming = lax.all_to_all(
        for_sending(before), SP, split_axis=0, concat_axis=3, tiled=True
    ).astype(before.dtype)[0]
    states = local_state + through[..., None] * incoming[None]
    query_blocks = queries.reshape(segment_count, SEGMENT_LENGTH, head_count, KEY_WIDTH)
    readout = jnp.einsum(
        "nshk,nhkv->nshv",
        query_blocks,
        states.astype(jnp.bfloat16),
        preferred_element_type=jnp.float32,
    )
    norm_scale = lax.rsqrt(jnp.mean(readout * readout, axis=-1, keepdims=True) + epsilon)
    gla_mix = (
        (readout * norm_scale * gla_gain)
        .astype(jnp.bfloat16)
        .reshape(row_count, head_count * HEAD_V)
    )
    reach_rows = conv_taps.shape[0] - 1
    earlier_rows = from_behind(conv_input[row_count - reach_rows :], SP, 1)
    extended = jnp.concatenate([earlier_rows, conv_input], axis=0)
    convolved = jnp.zeros(conv_input.shape, jnp.float32)
    for offset in range(reach_rows + 1):
        convolved = convolved + conv_taps[offset] * extended[offset : offset + row_count]
    conv_mix = (conv_gate * convolved).astype(jnp.bfloat16)
    wide_gla, wide_conv = turned_gather((out_gla, out_conv), SP, (1, 1))
    summed = jnp.dot(gla_mix, wide_gla, preferred_element_type=jnp.float32)
    mixed_rows = sent_and_summed(
        (summed + jnp.dot(conv_mix, wide_conv, preferred_element_type=jnp.float32)).astype(
            jnp.bfloat16
        ),
        "tp",
        0,
    )
    return mixed_rows.astype(jnp.bfloat16)


def solution(mesh):
    split = Mesh(mesh.devices.reshape(16, 4, 2, mesh.shape["tp"]), ("sp_0", "sp_1", "sp_2", "tp"))
    placed = (
        P(SP, "tp"),
        P(SP, "tp"),
        P(SP, "tp"),
        P(SP, None),
        P(None, "tp"),
        P("tp"),
        P(),
        P(SP, "tp"),
        P(SP, "tp"),
        P(None, "tp"),
        P("tp", SP),
        P("tp", SP),
    )
    return jax.shard_map(
        per_device, mesh=split, in_specs=placed, out_specs=P(SP_TP, None), check_vma=False
    )
```

profile of v0, /device:TPU:1, one launch (start us, length us, event | category | flops | bytes accessed | tf_op | source)
XLA Modules:
  0.0 189.0 jit_solution(4269959149335231402)
XLA Ops:
  6.5 1.4 pad_maximum_fusion.6
  7.9 0.0 all-gather.5.cloned.1.call-update
  8.0 1.1 fusion.12
  9.0 0.1 reshape.75
  9.2 0.1 fusion.36
  9.4 0.1 reshape.83
  9.5 0.1 reshape.76
  9.6 0.2 multiply_convert_fusion.3
  9.8 0.3 fusion.14
  10.1 0.1 slice_add_fusion
  10.3 0.1 fusion.32
  10.4 0.1 fusion.31
  10.5 0.1 pad.73
  10.7 0.1 pad.74
  10.9 0.1 copy.69
  11.0 0.1 copy.70
  11.1 10.3 %all_to_all.24 = bf16[64,2,1,2,128,2]{4,5,0,3,2,1:T(2,128)(2,1)S(1)} all-to-all(bf16[64,2,1,2,128,2]{4,5,0,3,2,1:T(2,128)(2,1)S(1)} %copy.70), channel_id=1, replica_groups=mesh['sp_0'=16,'sp_1'=4,'sp_2'=2,'tp'=4] {'sp_2'}, dimensions={1} | all-to-all | bytes 262144 | tf_op jit(solution)/shard_map/all_to_all | solution.py:34
  21.4 0.7 copy.71
  22.2 12.9 %all-to-all-start.1 = ((bf16[64,2,1,2,128,2]{4,5,1,3,2,0:T(2,128)(2,1)}), bf16[64,2,1,2,128,2]{4,5,1,3,2,0:T(2,128)(2,1)S(1)}, u32[]{:S(2)}, u32[]{:S(2)}) async-start(bf16[64,2,1,2,128,2]{4,5,1,3,2,0:T(2,128)(2,1)} %copy.71), calls=%async_computation.1 | async-start | bytes 262144 | tf_op jit(solution)/shard_map/all_to_all | solution.py:34
  35.2 25.6 %all-gather = f32[16,2,128]{2,1,0:T(2,128)S(1)} all-gather(f32[1,2,128]{2,1,0:T(2,128)S(1)} %slice_add_fusion.4), channel_id=2, replica_groups=mesh['sp_0'=16,'sp_1'=4,'sp_2'=2,'tp'=4] {'sp_0'}, dimensions={0}, use_global_device_ids=true | all-gather | bytes 17408 | tf_op jit(solution)/shard_map/all_gather | solution.py:47
  60.8 10.3 %all-gather.1 = f32[64,2,128]{2,1,0:T(2,128)S(1)} all-gather(f32[16,2,128]{2,1,0:T(2,128)S(1)} %all-gather), channel_id=3, replica_groups=mesh['sp_0'=16,'sp_1'=4,'sp_2'=2,'tp'=4] {'sp_1'}, dimensions={0}, use_global_device_ids=true | all-gather | bytes 81920 | tf_op jit(solution)/shard_map/all_gather | solution.py:47
  71.1 9.7 %all-gather.2 = f32[128,2,128]{2,1,0:T(2,128)S(1)} all-gather(f32[64,2,128]{2,1,0:T(2,128)S(1)} %all-gather.1), channel_id=4, replica_groups=mesh['sp_0'=16,'sp_1'=4,'sp_2'=2,'tp'=4] {'sp_2'}, dimensions={0}, use_global_device_ids=true | all-gather | bytes 196608 | tf_op jit(solution)/shard_map/all_gather | solution.py:47
  80.8 0.1 copy.74
  81.4 0.2 copy.73
  81.6 0.1 slice.267
  81.7 0.1 slice.268
  81.8 0.1 slice.273
  81.9 0.1 slice.274
  82.0 0.1 slice.279
  82.0 0.1 slice.280
  82.1 0.1 slice.285
  82.2 0.1 slice.286
  82.3 0.1 slice.291
  82.4 0.1 slice.292
  82.5 0.1 slice.297
  82.6 0.1 slice.298
  82.6 0.1 slice.306
  82.7 0.1 slice.308
  82.8 0.1 slice.310
  82.9 0.1 slice.312
  83.0 0.1 slice.314
  83.2 0.1 pad.81
  83.3 0.1 pad.82
  83.8 0.0 copy-start.4
  84.0 0.1 pad.190
  84.1 0.1 pad.116
  84.2 0.1 copy.80
  84.3 0.8 concatenate.41.clone
  85.1 13.7 %all-to-all-start.2 = ((bf16[128,2,128,2]{2,3,1,0:T(2,128)(2,1)}), bf16[128,2,128,2]{2,3,1,0:T(2,128)(2,1)S(1)}, u32[]{:S(2)}, u32[]{:S(2)}) async-start(bf16[128,2,128,2]{2,3,1,0:T(2,128)(2,1)} %concatenate.41.clone), calls=%async_computation.2 | async-start | bytes 262144 | tf_op jit(solution)/shard_map/all_to_all | solution.py:127
  98.8 3.5 %collective-permute-start = (bf16[2,512]{1,0:T(2,128)(2,1)S(1)}, bf16[2,512]{1,0:T(2,128)(2,1)S(1)}, u32[]{:S(2)}, u32[]{:S(2)}) collective-permute-start(bf16[2,512]{1,0:T(2,128)(2,1)S(1)} %slice.318), channel_id=1, source_target_pairs={{0,4},{4,8},{8,12},{12,16},{16,20},{20,24},{24,28},{28,32},{32,36}... | collective-permute-start | bytes 6152 | tf_op jit(solution)/shard_map/ppermute | solution.py:65
  102.5 12.7 %all-to-all-done.2 = bf16[128,2,128,2]{2,3,1,0:T(2,128)(2,1)S(1)} async-done(((bf16[128,2,128,2]{2,3,1,0:T(2,128)(2,1)}), bf16[128,2,128,2]{2,3,1,0:T(2,128)(2,1)S(1)}, u32[]{:S(2)}, u32[]{:S(2)}) %all-to-all-start.2) | async-done | bytes 131104 | tf_op jit(solution)/shard_map/all_to_all | solution.py:127
  115.1 0.1 convert_bitcast_fusion
  115.2 0.1 copy.76
  115.3 0.1 copy.77
  115.5 0.5 multiply_reduce_fusion
  115.9 0.1 multiply_convert_fusion.1
  116.1 0.3 copy.79
  116.4 42.7 %all-gather.5.cloned.1.call-done = bf16[2048,1024]{1,0:T(8,128)(2,1)} async-done(((bf16[16,1024]{1,0:T(8,128)(2,1)}), bf16[2048,1024]{1,0:T(8,128)(2,1)}) %all-gather.5.cloned.1.call-update) | async-done | bytes 4194320 | tf_op jit(solution)/shard_map/all_gather | solution.py:71
  159.1 2.5 %fusion.2 = f32[256,2048]{1,0:T(8,128)S(1)} fusion(bf16[256,512]{1,0:T(8,128)(2,1)S(1)} %bitcast.45, bf16[2048,1024]{1,0:T(8,128)(2,1)} %all-gather.5.cloned.1.call-done), kind=kOutput, calls=%fused_computation.3 | convolution fusion | flops 536870912 | bytes 4456448 | tf_op jit(solution)/shard_map/dot_general | solution.py:152
  161.6 0.3 copy-done.1
  161.9 0.0 copy-done.8
  162.0 0.9 fusion
  162.8 18.4 %all_to_all.25 = bf16[4,64,2048]{2,1,0:T(8,128)(2,1)S(1)} all-to-all(bf16[4,64,2048]{2,1,0:T(8,128)(2,1)S(1)} %bitcast.46), channel_id=1, replica_groups=mesh['sp_0'=16,'sp_1'=4,'sp_2'=2,'tp'=4] {'tp'}, dimensions={0} | all-to-all | bytes 2097152 | tf_op jit(solution)/shard_map/all_to_all | solution.py:81
  181.3 0.9 reduce_sum.22
  (101 shorter events, 1.3 us)
Async XLA Ops:
  6.5 1.4 copy-start
  6.5 2.8 %copy-start.3 = (bf16[256,256]{1,0:T(8,128)(2,1)S(1)}, bf16[256,256]{1,0:T(8,128)(2,1)}, u32[]{:S(2)}) copy-start(bf16[256,256]{1,0:T(8,128)(2,1)} %param.13) | copy-start | bytes 393220
  6.5 3.0 %copy-start.2 = (bf16[256,512]{1,0:T(8,128)(2,1)S(1)}, bf16[256,512]{1,0:T(8,128)(2,1)}, u32[]{:S(2)}) copy-start(bf16[256,512]{1,0:T(8,128)(2,1)} %param.14) | copy-start | bytes 786436
  6.5 152.6 %all-gather.5.cloned.1.call-start = ((), (), s32[]{:S(2)}) async-start(), calls=%async_computation.4 | async-start | bytes 4227072 | tf_op jit(solution)/shard_map/all_gather | solution.py:71
  22.2 59.1 %all-to-all-start.1 = ((bf16[64,2,1,2,128,2]{4,5,1,3,2,0:T(2,128)(2,1)}), bf16[64,2,1,2,128,2]{4,5,1,3,2,0:T(2,128)(2,1)S(1)}, u32[]{:S(2)}, u32[]{:S(2)}) async-start(bf16[64,2,1,2,128,2]{4,5,1,3,2,0:T(2,128)(2,1)} %copy.71), calls=%async_computation.1 | async-start | bytes 262144 | tf_op jit(solution)/shard_map/all_to_all | solution.py:34
  83.8 15.0 %copy-start.7 = (bf16[256,512]{1,0:T(8,128)(2,1)S(1)}, bf16[256,512]{1,0:T(8,128)(2,1)}, u32[]{:S(2)}) copy-start(bf16[256,512]{1,0:T(8,128)(2,1)} %param.19) | copy-start | bytes 786436
  83.8 18.6 %copy-start.4 = (bf16[256,256]{1,0:T(8,128)(2,1)S(1)}, bf16[256,256]{1,0:T(8,128)(2,1)}, u32[]{:S(2)}) copy-start(bf16[256,256]{1,0:T(8,128)(2,1)} %param.12) | copy-start | bytes 393220
  83.8 18.6 %copy-start.5 = (f32[3,512]{1,0:T(4,128)S(1)}, f32[3,512]{1,0:T(4,128)}, u32[]{:S(2)}) copy-start(f32[3,512]{1,0:T(4,128)} %param.21) | copy-start | bytes 18436
  85.1 30.0 %all-to-all-start.2 = ((bf16[128,2,128,2]{2,3,1,0:T(2,128)(2,1)}), bf16[128,2,128,2]{2,3,1,0:T(2,128)(2,1)S(1)}, u32[]{:S(2)}, u32[]{:S(2)}) async-start(bf16[128,2,128,2]{2,3,1,0:T(2,128)(2,1)} %concatenate.41.clone), calls=%async_computation.2 | async-start | bytes 262144 | tf_op jit(solution)/shard_map/all_to_all | solution.py:127
  98.8 62.8 %collective-permute-start = (bf16[2,512]{1,0:T(2,128)(2,1)S(1)}, bf16[2,512]{1,0:T(2,128)(2,1)S(1)}, u32[]{:S(2)}, u32[]{:S(2)}) collective-permute-start(bf16[2,512]{1,0:T(2,128)(2,1)S(1)} %slice.318), channel_id=1, source_target_pairs={{0,4},{4,8},{8,12},{12,16},{16,20},{20,24},{24,28},{28,32},{32,36}... | collective-permute-start | bytes 6152 | tf_op jit(solution)/shard_map/ppermute | solution.py:65
  115.2 0.7 copy-start.6
  159.1 2.8 %copy-start.1 = (bf16[2048,1024]{1,0:T(8,128)(2,1)S(1)}, bf16[2048,1024]{1,0:T(8,128)(2,1)}, u32[]{:S(2)}) copy-start(bf16[2048,1024]{1,0:T(8,128)(2,1)} %all-gather.5.cloned.1.call-done) | copy-start | bytes 12582916
  159.1 2.8 %copy-start.8 = (bf16[256,512]{1,0:T(8,128)(2,1)S(1)}, bf16[256,512]{1,0:T(8,128)(2,1)}, u32[]{:S(2)}) copy-start(bf16[256,512]{1,0:T(8,128)(2,1)} %param.20) | copy-start | bytes 786436
Sparse Core Ops, SparseCore 0:
  10.5 148.5 all-gather.4
where the time goes:
time: 189 us
  blocking collectives  74.3 us (39%)
  waiting for transfers between devices  55.4 us (29%)
  starting transfers between devices  30.2 us (16%)
  between operations  14.3 us (8%)
  local copies, waits for them, and re-layouts  5.91 us (3%)
  matrix products  5.23 us (3%)
  other arithmetic  3.7 us (2%)
    all_gather x3, blocking collectives, all_blocks(): parts = lax.all_gather(parts, axes[k], axis=0, tiled=True)  45.6 us
    all_gather x1, waiting for transfers between devices, turned_gather(): out, at, outs = (lax.all_gather(both, axis, axis=0, tiled=True), 0, [])  42.7 us
    all_to_all x1, blocking collectives, sent_and_summed(): lax.all_to_all(parts, axis, split_axis=0, concat_axis=0, tiled=True)  18.4 us
    all_to_all x1, starting transfers between devices, per_device(): lax.all_to_all(for_sending(before), SP, split_axis=0, concat_axis=3, tile...  13.7 us
    all_to_all x1, starting transfers between devices, turned_blocks(): out = lax.all_to_all(out, axes[k], k, k, tiled=True)  12.9 us
    all_to_all x1, waiting for transfers between devices, per_device(): lax.all_to_all(for_sending(before), SP, split_axis=0, concat_axis=3, tile...  12.7 us
    all_to_all x1, blocking collectives, turned_blocks(): out = lax.all_to_all(out, axes[k], k, k, tiled=True)  10.3 us
  transfers between devices with their start and end apart: 4, of which 2 were waited for; matrix products, arithmetic and copies ran while one was open for 6% of the time, Pallas kernels for 0%

commit v1 on v0

v1 whole, which is shorter than its diff:
```python
import functools

import jax
import jax.numpy as jnp
from jax import lax
from jax.experimental import pallas as pl
from jax.experimental.pallas import tpu as pltpu
from jax.sharding import PartitionSpec as P

MESH = pl.DeviceIdType.MESH
F32, BF16 = jnp.float32, jnp.bfloat16

NX, NC = 4, 2
KW, HV, SEG = 128, 256, 64
HEADS = 2
ROWS = 256
SEGS = ROWS // SEG
NCHUNK = 8
CW = 256
ORDER = (0, 1, -1, 2, -2, 3, -3, 4)
X_ORDER = (1, 3, 2)
NEAR = (1, 2, 3, 5, 6)
A_SEND = (1, 2, -1, -2, -3)
B_SEND = (5, 10)
NT = (((1,), (1,)), ((), ()))
TN = (((0,), (0,)), ((), ()))


def terms(a):
    high = a.astype(BF16).astype(F32)
    rest = a - high
    mid = rest.astype(BF16).astype(F32)
    return [high, mid, rest - mid]


def decay_rows(*decays):
    rows = [r for a in decays for r in terms(a)]
    rows.append(jnp.zeros((16 - len(rows), KW), F32))
    return jnp.concatenate(rows, axis=0).astype(BF16)


def decay_of(block, which=0):
    b = block.astype(F32)
    i = 3 * which
    return b[i : i + 1] + b[i + 1 : i + 2] + b[i + 2 : i + 3]


def chain(earlier, latter):
    return earlier[0] * latter[0], latter[0] * earlier[1] + latter[1]


def only_if(valid, pair):
    return jnp.where(valid, pair[0], 1.0), jnp.where(valid, pair[1], 0.0)


def layer_kernel(
    nz,
    nt,
    q, k, v, code, up, bias, gain, cin, cgate, taps, wblk,
    out,
    wt, states, through, ubuf, u0, pbuf, prec, abuf, arec, wbuf, brec, rbuf, sin,
    ctail, ext, mix, part, rel, comb, from_left, from_right,
    zsem, fsem, xs_sem, rs_sem, ls_sem, fs_sem, wd_sem,
    u0_sem, p_sem, a_sem, b_sem, r_sem, sin_sem, c_sem,
    rel_sem, left_sem, right_sem, tail_send,
):
    s = lax.axis_index("sp")
    t = lax.axis_index("tp")
    ns = nz * NX * NC
    c = lax.rem(s, NC)
    x = lax.rem(s // NC, NX)
    z = s // (NC * NX)

    def chip(zz, xx, cc):
        return {"sp": (zz * NX + xx) * NC + cc, "tp": t}

    def along_z(d):
        return chip(lax.rem(z + d + nz, nz), x, c)

    def along_x(d):
        return chip(z, lax.rem(x + d + NX, NX), c)

    def along_y(d):
        return {"sp": s, "tp": lax.rem(t + d + nt, nt)}

    def next_in_order(d):
        return {"sp": lax.rem(s + d + ns, ns), "tp": t}

    partner = chip(z, x, 1 - c)

    def rdma(src, dst, send, recv, dev):
        return pltpu.make_async_remote_copy(
            src_ref=src, dst_ref=dst, send_sem=send, recv_sem=recv,
            device_id=dev, device_id_type=MESH,
        )

    barrier = pltpu.get_barrier_semaphore()

    def greet(dev):
        pl.semaphore_signal(barrier, inc=1, device_id=dev, device_id_type=MESH)

    greet(partner)
    for d in (1, 2, 3):
        greet(along_x(d))
    for d in (1, -1):
        greet(along_y(d))
        greet(next_in_order(d))

    @pl.when(c == 0)
    def _():
        greet(along_z(1))
        greet(along_z(-1))

    @pl.when(c == 1)
    def _():
        for d in NEAR:
            greet(along_z(d))
            greet(along_z(-d))

    score = jnp.dot(code[...], up[...], preferred_element_type=F32) + bias[...]
    log_decay = (jnp.minimum(score, 0.0) - jnp.log1p(jnp.exp(-jnp.abs(score)))) / 16.0
    row = lax.broadcasted_iota(jnp.int32, (SEG, SEG), 0)
    col = lax.broadcasted_iota(jnp.int32, (SEG, SEG), 1)
    later = (col > row).astype(F32)
    acc = [None] * HEADS
    thr = None
    for n in range(SEGS):
        here = log_decay[n * SEG : (n + 1) * SEG]
        rest = jnp.dot(
            later, here, preferred_element_type=F32, precision=lax.Precision.HIGHEST
        )
        scaled = (k[n * SEG : (n + 1) * SEG, :].astype(F32) * jnp.exp(rest)).astype(BF16)
        seg_decay = jnp.exp(rest[0:1] + here[0:1])
        thr = seg_decay if n == 0 else thr * seg_decay
        through[n] = jnp.broadcast_to(thr, (8, HEADS * KW))
        for h in range(HEADS):
            update = lax.dot_general(
                v[n * SEG : (n + 1) * SEG, h * HV : (h + 1) * HV],
                scaled[:, h * KW : (h + 1) * KW],
                TN,
                preferred_element_type=F32,
            )
            if n == 0:
                acc[h] = update
            else:
                acc[h] = acc[h] * seg_decay[:, h * KW : (h + 1) * KW] + update
            states[n, h * HV : (h + 1) * HV, :] = acc[h]
    for h in range(HEADS):
        ubuf[h * HV : (h + 1) * HV, :] = acc[h].astype(BF16)
    ubuf[HEADS * HV :, :] = decay_rows(thr[:, :KW], thr[:, KW:])

    @pl.when(c == 0)
    def _():
        wt[z, x, 0:16, :] = wblk[...]
        pl.semaphore_wait(barrier, 10)

    @pl.when(c == 1)
    def _():
        pl.semaphore_wait(barrier, 18)

    tail_copy = rdma(
        cin.at[ROWS - 16 : ROWS], ctail, c_sem.at[0], c_sem.at[1], next_in_order(1)
    )

    def conv():
        tail_copy.wait_recv()
        ext[8:, :] = cin[...].astype(F32)
        ext[0:8, :] = jnp.where(s == 0, 0.0, ctail[...].astype(F32)[8:16])
        done = taps[0:1] * ext[6 : 6 + ROWS, :]
        done = done + taps[1:2] * ext[7 : 7 + ROWS, :]
        done = done + taps[2:3] * ext[8 : 8 + ROWS, :]
        mix[:, HEADS * HV :] = (cgate[...].astype(F32) * done).astype(BF16)

    def read_out(incoming):
        for h in range(HEADS):
            for n in range(SEGS):
                decay = through[n, 0:1, h * KW : (h + 1) * KW]
                state = states[n, h * HV : (h + 1) * HV, :] + decay * incoming(h)
                got = lax.dot_general(
                    q[n * SEG : (n + 1) * SEG, h * KW : (h + 1) * KW],
                    state.astype(BF16),
                    NT,
                    preferred_element_type=F32,
                )
                scale = lax.rsqrt(jnp.mean(got * got, axis=-1, keepdims=True) + 1.0)
                mix[n * SEG : (n + 1) * SEG, h * HV : (h + 1) * HV] = (
                    got * scale * gain[...]
                ).astype(BF16)

    def block_copy(rr, xx, send, dev):
        return rdma(wt.at[rr, xx], wt.at[rr, xx], send, zsem.at[rr, xx], dev)

    def pass_on(rr):
        rdma(wt.at[rr], wt.at[rr], fs_sem, fsem.at[rr], partner).start()

    def row_at(d):
        return lax.rem(z + d + nz, nz)

    @pl.when(c == 0)
    def _():
        rdma(ubuf, u0, u0_sem.at[0], u0_sem.at[1], partner).start()
        tail_copy.start()
        rdma(wblk, wt.at[z, x, 16:32], wd_sem.at[0], wd_sem.at[1], partner).wait_recv()
        for d in X_ORDER:
            block_copy(z, x, xs_sem, along_x(d)).start()
        block_copy(z, x, rs_sem, along_z(1)).start()
        block_copy(z, x, ls_sem, along_z(-1)).start()
        conv()
        for d in X_ORDER:
            xx = lax.rem(x + d, NX)
            block_copy(z, xx, xs_sem, along_x(d)).wait_recv()
            block_copy(z, xx, rs_sem, along_z(1)).start()
            block_copy(z, xx, ls_sem, along_z(-1)).start()
        pass_on(z)

        @pl.loop(1, nz // 2 - 1)
        def _(step):
            up_row, down_row = row_at(-step), row_at(step)
            for d in (0,) + X_ORDER:
                xx = lax.rem(x + d, NX)
                block_copy(up_row, xx, rs_sem, along_z(1)).wait_recv()
                block_copy(up_row, xx, rs_sem, along_z(1)).start()
                block_copy(down_row, xx, ls_sem, along_z(-1)).wait_recv()
                block_copy(down_row, xx, ls_sem, along_z(-1)).start()
            pass_on(up_row)
            pass_on(down_row)

        up_row, down_row = row_at(1 - nz // 2), row_at(nz // 2 - 1)
        for d in (0,) + X_ORDER:
            xx = lax.rem(x + d, NX)
            block_copy(up_row, xx, rs_sem, along_z(1)).wait_recv()
            block_copy(up_row, xx, rs_sem, along_z(1)).start()
            block_copy(down_row, xx, ls_sem, along_z(-1)).wait_recv()
        pass_on(up_row)
        pass_on(down_row)
        far = row_at(nz // 2)
        for d in (0,) + X_ORDER:
            block_copy(far, lax.rem(x + d, NX), rs_sem, along_z(1)).wait_recv()
        pass_on(far)

        rdma(sin, sin, sin_sem.at[0], sin_sem.at[1], partner).wait_recv()
        read_out(
            lambda h: jnp.concatenate([sin[2 * h], sin[2 * h + 1]], axis=0).astype(F32)
        )

    @pl.when(c == 1)
    def _():
        rdma(wblk, wt.at[z, x, 16:32], wd_sem.at[0], wd_sem.at[1], partner).start()
        tail_copy.start()
        rdma(ubuf, u0, u0_sem.at[0], u0_sem.at[1], partner).wait_recv()
        first = [decay_of(u0[HEADS * HV :, :], h) for h in range(HEADS)]
        whole = [thr[:, h * KW : (h + 1) * KW] * first[h] for h in range(HEADS)]
        for i in range(NX):
            h, lo = i // 2, i * KW
            both = (
                u0[lo : lo + KW, :].astype(F32) * thr[:, h * KW : (h + 1) * KW]
                + acc[h][(i % 2) * KW : (i % 2 + 1) * KW]
            )
            pbuf[i, 0:KW, :] = both.astype(BF16)
            pbuf[i, KW:, :] = decay_rows(whole[h])
        for j, d in enumerate((1, 3, 2)):
            rdma(
                pbuf.at[lax.rem(x + d, NX)], prec.at[x],
                p_sem.at[0], p_sem.at[1 + d], along_x(d),
            ).start()
        prec[x] = pbuf[x]
        for d in (1, 2, 3):
            rdma(
                pbuf.at[0], prec.at[lax.rem(x - d + NX, NX)],
                p_sem.at[0], p_sem.at[1 + d], along_x(d),
            ).wait_recv()

        def pair_in(ref, i):
            return decay_of(ref[i, KW:, :]), ref[i, 0:KW, :].astype(F32)

        chips = [pair_in(prec, i) for i in range(NX)]
        plane = chips[0]
        for i in range(1, NX):
            plane = chain(plane, chips[i])
        abuf[0:KW, :] = plane[1].astype(BF16)
        abuf[KW:, :] = decay_rows(plane[0])
        for j, d in enumerate(A_SEND):
            rdma(abuf, arec.at[j], a_sem.at[5], a_sem.at[j], along_z(d)).start()
        conv()
        for j, d in enumerate(A_SEND):
            rdma(abuf, arec.at[j], a_sem.at[5], a_sem.at[j], along_z(d)).wait_recv()
        back1, back2, ahead1, ahead2, ahead3 = (pair_in(arec, j) for j in range(5))
        inner = z <= nz - 4
        window = only_if(inner & (z >= 2), back2)
        window = chain(window, only_if(inner & (z >= 1), back1))
        window = chain(window, only_if(inner, plane))
        window = chain(window, only_if(inner | (z == nz - 1), ahead1))
        window = chain(window, only_if(inner | (z >= nz - 2), ahead2))
        wbuf[0:KW, :] = window[1].astype(BF16)
        wbuf[KW:, :] = decay_rows(window[0])
        for j, d in enumerate(B_SEND):
            rdma(wbuf, brec.at[j], b_sem.at[2], b_sem.at[j], along_z(d)).start()
        oldest = only_if(z >= nz - 1, ahead1)
        oldest = chain(oldest, only_if(z >= nz - 2, ahead2))
        oldest = chain(oldest, only_if(z >= nz - 3, ahead3))
        newest = chain(only_if(z >= 2, back2), only_if(z >= 1, back1))
        for j, d in enumerate(B_SEND):
            rdma(wbuf, brec.at[j], b_sem.at[2], b_sem.at[j], along_z(d)).wait_recv()
        before = chain(oldest, only_if(z >= 8, pair_in(brec, 1)))
        before = chain(before, only_if(z >= 3, pair_in(brec, 0)))
        before = chain(before, newest)
        run = before[1]
        for i in range(NX):
            rbuf[i] = run.astype(BF16)
            if i < NX - 1:
                run = chips[i][0] * run + chips[i][1]
        for d in (1, 3, 2):
            rdma(
                rbuf.at[lax.rem(x + d, NX)], sin.at[x],
                r_sem.at[0], r_sem.at[1 + d], along_x(d),
            ).start()
        sin[x] = rbuf[x]
        for d in (1, 2, 3):
            rdma(
                rbuf.at[0], sin.at[lax.rem(x - d + NX, NX)],
                r_sem.at[0], r_sem.at[1 + d], along_x(d),
            ).wait_recv()
        rdma(sin, sin, sin_sem.at[0], sin_sem.at[1], partner).start()

        def incoming(h):
            got = jnp.concatenate([sin[2 * h], sin[2 * h + 1]], axis=0).astype(F32)
            return first[h] * got + u0[h * HV : (h + 1) * HV, :].astype(F32)

        read_out(incoming)

    right, left = along_y(1), along_y(-1)
    opposite, at_right, at_left = (lax.rem(t + d, nt) for d in (2, 1, 3))
    zc = z // 2
    columns = [lax.rem(zc + d + NCHUNK, NCHUNK) for d in ORDER]
    for o, j in enumerate(columns):
        @pl.when(c == 1)
        def _():
            for i in range(2):
                rdma(
                    wt.at[2 * j + i], wt.at[2 * j + i], fs_sem, fsem.at[2 * j + i], partner
                ).wait_recv()

        w = wt[pl.ds(2 * j, 2)].reshape(CW, 2 * HEADS * HV)
        got = lax.dot_general(mix[...], w, NT, preferred_element_type=F32)
        part[o] = got.astype(BF16).reshape(nt, ROWS // nt, CW)
        rdma(
            part.at[o, opposite], rel.at[o], tail_send.at[0], rel_sem.at[o],
            right if o % 2 == 0 else left,
        ).start()
    for o in range(NCHUNK):
        if o % 2 == 0:
            rdma(
                part.at[o, at_left], from_right.at[o], tail_send.at[1],
                right_sem.at[o], left,
            ).start()
        else:
            rdma(
                part.at[o, at_right], from_left.at[o], tail_send.at[1],
                left_sem.at[o], right,
            ).start()
    for o in range(NCHUNK):
        to = right if o % 2 == 0 else left
        rdma(part.at[o, 0], rel.at[o], tail_send.at[0], rel_sem.at[o], to).wait_recv()
        mine = part[o, at_right if o % 2 == 0 else at_left]
        comb[o] = (rel[o].astype(F32) + mine.astype(F32)).astype(BF16)
        if o % 2 == 0:
            rdma(comb.at[o], from_left.at[o], tail_send.at[2], left_sem.at[o], right).start()
        else:
            rdma(comb.at[o], from_right.at[o], tail_send.at[2], right_sem.at[o], left).start()
    for o, j in enumerate(columns):
        rdma(comb.at[o], from_left.at[o], tail_send.at[2], left_sem.at[o], right).wait_recv()
        rdma(comb.at[o], from_right.at[o], tail_send.at[2], right_sem.at[o], left).wait_recv()
        total = part[o, t].astype(F32) + from_left[o].astype(F32) + from_right[o].astype(F32)
        out[:, pl.ds(pl.multiple_of(j * CW, CW), CW)] = total.astype(BF16)

    for i in range(3):
        rdma(comb, rel, tail_send.at[i], rel_sem.at[0], right).wait_send()
    tail_copy.wait_send()

    @pl.when(c == 0)
    def _():
        rdma(ubuf, u0, u0_sem.at[0], u0_sem.at[1], partner).wait_send()
        rdma(wt.at[0, 0:3], wt.at[0, 0:3], xs_sem, zsem.at[0, 0], partner).wait_send()
        half = nz // 2
        rdma(wt.at[0:half], wt.at[0:half], rs_sem, zsem.at[0, 0], partner).wait_send()
        rdma(
            wt.at[0 : half - 1], wt.at[0 : half - 1], ls_sem, zsem.at[0, 0], partner
        ).wait_send()
        rdma(wt, wt, fs_sem, fsem.at[0], partner).wait_send()

    @pl.when(c == 1)
    def _():
        rdma(wblk, wt.at[0, 0, 0:16], wd_sem.at[0], wd_sem.at[1], partner).wait_send()
        rdma(pbuf.at[0:3], prec.at[0:3], p_sem.at[0], p_sem.at[1], partner).wait_send()
        rdma(arec, arec, a_sem.at[5], a_sem.at[0], partner).wait_send()
        rdma(brec, brec, b_sem.at[2], b_sem.at[0], partner).wait_send()
        rdma(rbuf.at[0:3], sin.at[0:3], r_sem.at[0], r_sem.at[1], partner).wait_send()
        rdma(sin, sin, sin_sem.at[0], sin_sem.at[1], partner).wait_send()


def solution(mesh):
    nt = mesh.shape["tp"]
    nz = mesh.shape["sp"] // (NX * NC)

    def step(
        queries, keys, values, gate_code, gate_up, gate_bias, gla_gain,
        conv_input, conv_gate, conv_taps, out_gla, out_conv,
    ):
        weights = jnp.concatenate([out_gla.T, out_conv.T], axis=1)
        width = HEADS * HV
        vm, dma = pltpu.VMEM, pltpu.SemaphoreType.DMA
        quarter = ROWS // nt
        scratch = [
            vm((nz, NX, 32, 2 * width), BF16),
            vm((SEGS, width, KW), F32),
            vm((SEGS, 8, HEADS * KW), F32),
            vm((width + 16, KW), BF16),
            vm((width + 16, KW), BF16),
            vm((NX, KW + 16, KW), BF16),
            vm((NX, KW + 16, KW), BF16),
            vm((KW + 16, KW), BF16),
            vm((5, KW + 16, KW), BF16),
            vm((KW + 16, KW), BF16),
            vm((2, KW + 16, KW), BF16),
            vm((NX, KW, KW), BF16),
            vm((NX, KW, KW), BF16),
            vm((16, width), BF16),
            vm((8 + ROWS, width), F32),
            vm((ROWS, 2 * width), BF16),
            vm((NCHUNK, nt, quarter, CW), BF16),
            vm((NCHUNK, quarter, CW), BF16),
            vm((NCHUNK, quarter, CW), BF16),
            vm((NCHUNK, quarter, CW), BF16),
            vm((NCHUNK, quarter, CW), BF16),
            dma((nz, NX)), dma((nz,)), dma, dma, dma, dma, dma((2,)),
            dma((2,)), dma((5,)), dma((6,)), dma((3,)), dma((5,)), dma((2,)), dma((2,)),
            dma((NCHUNK,)), dma((NCHUNK,)), dma((NCHUNK,)), dma((3,)),
        ]
        return pl.pallas_call(
            functools.partial(layer_kernel, nz, nt),
            out_shape=jax.ShapeDtypeStruct((quarter, 2048), BF16),
            in_specs=[pl.BlockSpec(memory_space=pltpu.VMEM)] * 11,
            out_specs=pl.BlockSpec(memory_space=pltpu.VMEM),
            scratch_shapes=scratch,
            compiler_params=pltpu.CompilerParams(collective_id=0, has_side_effects=True),
            name="layer",
        )(
            queries, keys, values, gate_code, gate_up, gate_bias[None], gla_gain[None],
            conv_input, conv_gate, conv_taps, weights,
        )

    return jax.shard_map(
        step,
        mesh=mesh,
        in_specs=(
            P("sp", "tp"), P("sp", "tp"), P("sp", "tp"), P("sp", None), P(None, "tp"),
            P("tp"), P(), P("sp", "tp"), P("sp", "tp"), P(None, "tp"),
            P("tp", "sp"), P("tp", "sp"),
        ),
        out_specs=P(("sp", "tp"), None),
        check_vma=False,
    )
```

time: 189 us -> 69.2 us (0.37)
  blocking collectives: 74.3 us -> 0 us
  Pallas kernels: 0 us -> 65.1 us
  waiting for transfers between devices: 55.4 us -> 0 us
  starting transfers between devices: 30.2 us -> 0 us
  between operations: 14.3 us -> 0.01 us
  matrix products: 5.23 us -> 0 us
  local copies, waits for them, and re-layouts: 5.91 us -> 2.41 us
  other arithmetic: 3.7 us -> 1.35 us
    pallas_call x0 -> x1, Pallas kernels: none -> 65.1 us  [step(): pl.pallas_call(functools.partial(layer_kernel, nz, nt), out_shape=jax.Sha...]
    all_gather x3 -> x0, blocking collectives: 45.6 us -> none  [all_blocks(): parts = lax.all_gather(parts, axes[k], axis=0, tiled=True)]
    all_gather x1 -> x0, waiting for transfers between devices: 42.7 us -> none  [turned_gather(): out, at, outs = (lax.all_gather(both, axis, axis=0, tiled=True), 0, [])]
    all_to_all x2 -> x0, blocking collectives: 28.7 us -> none  [the longest x1 18.4 us: sent_and_summed(): lax.all_to_all(parts, axis, split_axis=0, concat_axis=0, tiled=True)]
    all_to_all x2 -> x0, starting transfers between devices: 26.6 us -> none  [the longest x1 13.7 us: per_device(): lax.all_to_all(for_sending(before), SP, split_axis=0, concat_axis=3, tile...]
    all_to_all x2 -> x0, waiting for transfers between devices: 12.7 us -> none  [the longest x1 12.7 us: per_device(): lax.all_to_all(for_sending(before), SP, split_axis=0, concat_axis=3, tile...]
    dot_general x5 -> x0, matrix products: 5.23 us -> none  [the longest x1 2.47 us: per_device(): summed = jnp.dot(gla_mix, wide_gla, preferred_element_type=jnp.float32)]
    ppermute x1 -> x0, starting transfers between devices: 3.54 us -> none  [from_behind(): return lax.ppermute(x, axis, pairs)]
  transfers between devices with their start and end apart: 4 -> 0, of which waited for: 2 -> 0; matrix products, arithmetic and copies ran while one was open for 6% -> 0% of each run, Pallas kernels for 0% -> 0%
where the time goes in v1:
time: 69.2 us; the launch traced here: 68.9 us
  Pallas kernels  65.1 us (94%)
  local copies, waits for them, and re-layouts  2.41 us (3%)
  other arithmetic  1.35 us (2%)
    pallas_call x1, Pallas kernels, step(): pl.pallas_call(functools.partial(layer_kernel, nz, nt), out_shape=jax.Sha...  65.1 us
    unnamed x4, local copies, waits for them, and re-layouts  2.41 us

profile of v1, /device:TPU:1, one launch (start us, length us, event | category | flops | bytes accessed | tf_op | source)
XLA Modules:
  0.0 68.9 jit_solution(1658134278912517130)
XLA Ops:
  0.0 0.0 copy-start
  0.0 1.4 %pad_maximum_fusion.wblk = bf16[16,1024]{1,0:T(8,128)(2,1)} fusion(bf16[16,512]{1,0:T(8,128)(2,1)} %bitcast.4, bf16[16,512]{1,0:T(8,128)(2,1)} %bitcast.5), kind=kLoop, calls=%fused_computation | loop fusion | flops 65536 | bytes 65536 | tf_op jit(solution)/shard_map/concatenate | solution.py:409
  1.4 0.0 copy-done
  1.4 0.7 %copy.13.code = bf16[256,32]{1,0:T(8,128)(2,1)} copy(bf16[256,32]{0,1:T(8,128)(2,1)S(1)} %copy-done) | data formatting | bytes 32768 | tf_op args[3]
  2.1 65.1 %layer.1 = bf16[64,2048]{1,0:T(8,128)(2,1)} custom-call(bf16[256,256]{1,0:T(8,128)(2,1)} %q.1, bf16[256,256]{1,0:T(8,128)(2,1)} %k.1, bf16[256,512]{1,0:T(8,128)(2,1)} %v.1, bf16[256,32]{1,0:T(8,128)(2,1)} %copy.13.code, bf16[32,256]{1,0:T(8,128)(2,1)} %up.1, f32[1,256]{1,0:T(1,128)} %bitcast.6, f32[1,256]{1,0:T(1,128)} %bitcast.7, bf16[256,512]{1,0:T(8,128)(2,1)} %cin.1, ...), custom_call_target="tpu_custom_call" | custom-call | tf_op jit(solution)/shard_map/layer/pallas_call | solution.py:439
  67.2 1.7 %copy.15 = bf16[64,2048]{1,0:T(8,128)(2,1)} copy(bf16[64,2048]{1,0:T(8,128)(2,1)} %layer.1) | data formatting | bytes 524288
Async XLA Ops:
  0.0 1.4 %copy-start = (bf16[256,32]{0,1:T(8,128)(2,1)S(1)}, bf16[256,32]{0,1:T(8,128)(2,1)}, u32[]{:S(2)}) copy-start(bf16[256,32]{0,1:T(8,128)(2,1)} %param.15) | copy-start | bytes 49156

commit v2 on v1

--- a/solution.py
+++ b/solution.py
@@ -17,11 +17,18 @@
 SEGS = ROWS // SEG
 NCHUNK = 8
 CW = 256
+W, S = 1, 0
 ORDER = (0, 1, -1, 2, -2, 3, -3, 4)
 X_ORDER = (1, 3, 2)
 NEAR = (1, 2, 3, 5, 6)
 A_SEND = (1, 2, -1, -2, -3)
 B_SEND = (5, 10)
+Z_SENDS = {
+    0: (1, -1, 5, -5), 5: (1, -1), -5: (1, -1), -1: (1,), 1: (-1,),
+    4: (1,), 6: (-1,), 7: (-1,), -6: (1,), -4: (-1,),
+}
+ARRIVE_ORDER = (1, -1, 5, -5, 2, -2, 4, 6, -4, -6, 3, 7, -3, -7, 8)
+LAG_R, LAG_F = 4, 7
 NT = (((1,), (1,)), ((), ()))
 TN = (((0,), (0,)), ((), ()))
 
@@ -56,11 +63,11 @@
 def layer_kernel(
     nz,
     nt,
-    q, k, v, code, up, bias, gain, cin, cgate, taps, wblk,
+    q, k, v, code, up, bias, gain, cin, cgate, taps, wgla, wconv,
     out,
     wt, states, through, ubuf, u0, pbuf, prec, abuf, arec, wbuf, brec, rbuf, sin,
-    ctail, ext, mix, part, rel, comb, from_left, from_right,
-    zsem, fsem, xs_sem, rs_sem, ls_sem, fs_sem, wd_sem,
+    ctail, ext, mix, wblk, sout, part, rel, comb, from_left, from_right,
+    zsem, fsem, ws_sem, fs_sem, wd_sem,
     u0_sem, p_sem, a_sem, b_sem, r_sem, sin_sem, c_sem,
     rel_sem, left_sem, right_sem, tail_send,
 ):
@@ -106,18 +113,19 @@
         greet(along_y(d))
         greet(next_in_order(d))
 
-    @pl.when(c == 0)
-    def _():
-        greet(along_z(1))
-        greet(along_z(-1))
-
-    @pl.when(c == 1)
+    @pl.when(c == W)
+    def _():
+        for d in (1, 5):
+            greet(along_z(d))
+            greet(along_z(-d))
+
+    @pl.when(c == S)
     def _():
         for d in NEAR:
             greet(along_z(d))
             greet(along_z(-d))
 
-    score = jnp.dot(code[...], up[...], preferred_element_type=F32) + bias[...]
+    score = lax.dot_general(code[...], up[...], TN, preferred_element_type=F32) + bias[...]
     log_decay = (jnp.minimum(score, 0.0) - jnp.log1p(jnp.exp(-jnp.abs(score)))) / 16.0
     row = lax.broadcasted_iota(jnp.int32, (SEG, SEG), 0)
     col = lax.broadcasted_iota(jnp.int32, (SEG, SEG), 1)
@@ -149,12 +157,16 @@
         ubuf[h * HV : (h + 1) * HV, :] = acc[h].astype(BF16)
     ubuf[HEADS * HV :, :] = decay_rows(thr[:, :KW], thr[:, KW:])
 
-    @pl.when(c == 0)
-    def _():
-        wt[z, x, 0:16, :] = wblk[...]
-        pl.semaphore_wait(barrier, 10)
-
-    @pl.when(c == 1)
+    own_rows, other_rows = slice(16 * W, 16 * W + 16), slice(16 * S, 16 * S + 16)
+    wblk[:, : HEADS * HV] = wgla[...]
+    wblk[:, HEADS * HV :] = wconv[...]
+
+    @pl.when(c == W)
+    def _():
+        wt[z, x, own_rows, :] = wblk[...]
+        pl.semaphore_wait(barrier, 12)
+
+    @pl.when(c == S)
     def _():
         pl.semaphore_wait(barrier, 18)
 
@@ -187,77 +199,82 @@
                     got * scale * gain[...]
                 ).astype(BF16)
 
-    def block_copy(rr, xx, send, dev):
-        return rdma(wt.at[rr, xx], wt.at[rr, xx], send, zsem.at[rr, xx], dev)
-
-    def pass_on(rr):
-        rdma(wt.at[rr], wt.at[rr], fs_sem, fsem.at[rr], partner).start()
+    def arrived(h):
+        return jnp.concatenate([sin[2 * h], sin[2 * h + 1]], axis=0).astype(F32)
+
+    def send_block(rr, xx, sem, dev):
+        block = wt.at[rr, xx]
+        rdma(block, block, ws_sem.at[sem], zsem.at[rr, xx], dev).start()
+
+    def wait_block(rr, xx):
+        block = wt.at[rr, xx]
+        rdma(block, block, ws_sem.at[0], zsem.at[rr, xx], partner).wait_recv()
 
     def row_at(d):
         return lax.rem(z + d + nz, nz)
 
-    @pl.when(c == 0)
+    def x_at(d):
+        return lax.rem(x + d, NX)
+
+    def arrive(d):
+        if d != 0:
+            wait_block(row_at(d), x)
+        for to in Z_SENDS.get(d, ()):
+            send_block(row_at(d), x, 0, along_z(to))
+        for to in (1, 3):
+            send_block(row_at(d), x, 1, along_x(to))
+
+    def relay(d):
+        near = 3 if d <= 0 else 1
+        wait_block(row_at(d), x_at(near))
+        send_block(row_at(d), x_at(near), 2, along_x(4 - near))
+
+    def finish(d):
+        far = 1 if d <= 0 else 3
+        wait_block(row_at(d), x_at(far))
+        wait_block(row_at(d), x_at(2))
+        rr = row_at(d)
+        rdma(wt.at[rr], wt.at[rr], fs_sem, fsem.at[rr], partner).start()
+
+    @pl.when(c == W)
     def _():
         rdma(ubuf, u0, u0_sem.at[0], u0_sem.at[1], partner).start()
         tail_copy.start()
-        rdma(wblk, wt.at[z, x, 16:32], wd_sem.at[0], wd_sem.at[1], partner).wait_recv()
-        for d in X_ORDER:
-            block_copy(z, x, xs_sem, along_x(d)).start()
-        block_copy(z, x, rs_sem, along_z(1)).start()
-        block_copy(z, x, ls_sem, along_z(-1)).start()
+        rdma(wblk, wt.at[z, x, other_rows], wd_sem.at[0], wd_sem.at[1], partner).wait_recv()
+        arrive(0)
         conv()
-        for d in X_ORDER:
-            xx = lax.rem(x + d, NX)
-            block_copy(z, xx, xs_sem, along_x(d)).wait_recv()
-            block_copy(z, xx, rs_sem, along_z(1)).start()
-            block_copy(z, xx, ls_sem, along_z(-1)).start()
-        pass_on(z)
-
-        @pl.loop(1, nz // 2 - 1)
-        def _(step):
-            up_row, down_row = row_at(-step), row_at(step)
-            for d in (0,) + X_ORDER:
-                xx = lax.rem(x + d, NX)
-                block_copy(up_row, xx, rs_sem, along_z(1)).wait_recv()
-                block_copy(up_row, xx, rs_sem, along_z(1)).start()
-                block_copy(down_row, xx, ls_sem, along_z(-1)).wait_recv()
-                block_copy(down_row, xx, ls_sem, along_z(-1)).start()
-            pass_on(up_row)
-            pass_on(down_row)
-
-        up_row, down_row = row_at(1 - nz // 2), row_at(nz // 2 - 1)
-        for d in (0,) + X_ORDER:
-            xx = lax.rem(x + d, NX)
-            block_copy(up_row, xx, rs_sem, along_z(1)).wait_recv()
-            block_copy(up_row, xx, rs_sem, along_z(1)).start()
-            block_copy(down_row, xx, ls_sem, along_z(-1)).wait_recv()
-        pass_on(up_row)
-        pass_on(down_row)
-        far = row_at(nz // 2)
-        for d in (0,) + X_ORDER:
-            block_copy(far, lax.rem(x + d, NX), rs_sem, along_z(1)).wait_recv()
-        pass_on(far)
-
+        order = (0,) + ARRIVE_ORDER
+        for i in range(1, nz + LAG_F):
+            if i < nz:
+                arrive(order[i])
+            if 0 <= i - LAG_R < nz:
+                relay(order[i - LAG_R])
+            if 0 <= i - LAG_F < nz:
+                finish(order[i - LAG_F])
         rdma(sin, sin, sin_sem.at[0], sin_sem.at[1], partner).wait_recv()
-        read_out(
-            lambda h: jnp.concatenate([sin[2 * h], sin[2 * h + 1]], axis=0).astype(F32)
-        )
-
-    @pl.when(c == 1)
-    def _():
-        rdma(wblk, wt.at[z, x, 16:32], wd_sem.at[0], wd_sem.at[1], partner).start()
+        read_out(arrived)
+
+    @pl.when(c == S)
+    def _():
+        rdma(wblk, wt.at[z, x, other_rows], wd_sem.at[0], wd_sem.at[1], partner).start()
         tail_copy.start()
         rdma(ubuf, u0, u0_sem.at[0], u0_sem.at[1], partner).wait_recv()
-        first = [decay_of(u0[HEADS * HV :, :], h) for h in range(HEADS)]
-        whole = [thr[:, h * KW : (h + 1) * KW] * first[h] for h in range(HEADS)]
+
+        def theirs(h, lo, hi):
+            return (
+                decay_of(u0[HEADS * HV :, :], h),
+                u0[h * HV + lo : h * HV + hi, :].astype(F32),
+            )
+
+        def ours(h, lo, hi):
+            return thr[:, h * KW : (h + 1) * KW], acc[h][lo:hi]
+
+        first, second = (theirs, ours) if S == 1 else (ours, theirs)
         for i in range(NX):
-            h, lo = i // 2, i * KW
-            both = (
-                u0[lo : lo + KW, :].astype(F32) * thr[:, h * KW : (h + 1) * KW]
-                + acc[h][(i % 2) * KW : (i % 2 + 1) * KW]
-            )
-            pbuf[i, 0:KW, :] = both.astype(BF16)
-            pbuf[i, KW:, :] = decay_rows(whole[h])
+            part_of = (i // 2, (i % 2) * KW, (i % 2 + 1) * KW)
+            both = chain(first(*part_of), second(*part_of))
+            pbuf[i, 0:KW, :] = both[1].astype(BF16)
+            pbuf[i, KW:, :] = decay_rows(both[0])
         for j, d in enumerate((1, 3, 2)):
             rdma(
                 pbuf.at[lax.rem(x + d, NX)], prec.at[x],
@@ -320,20 +337,25 @@
                 rbuf.at[0], sin.at[lax.rem(x - d + NX, NX)],
                 r_sem.at[0], r_sem.at[1 + d], along_x(d),
             ).wait_recv()
-        rdma(sin, sin, sin_sem.at[0], sin_sem.at[1], partner).start()
-
-        def incoming(h):
-            got = jnp.concatenate([sin[2 * h], sin[2 * h + 1]], axis=0).astype(F32)
-            return first[h] * got + u0[h * HV : (h + 1) * HV, :].astype(F32)
-
-        read_out(incoming)
+
+        def after_first(h):
+            decay, update = first(h, 0, HV)
+            return decay * arrived(h) + update
+
+        if S == 1:
+            rdma(sin, sin, sin_sem.at[0], sin_sem.at[1], partner).start()
+        else:
+            for h in range(HEADS):
+                sout[2 * h : 2 * h + 2] = after_first(h).astype(BF16).reshape(2, KW, KW)
+            rdma(sout, sin, sin_sem.at[0], sin_sem.at[1], partner).start()
+        read_out(after_first if S == 1 else arrived)
 
     right, left = along_y(1), along_y(-1)
     opposite, at_right, at_left = (lax.rem(t + d, nt) for d in (2, 1, 3))
     zc = z // 2
     columns = [lax.rem(zc + d + NCHUNK, NCHUNK) for d in ORDER]
     for o, j in enumerate(columns):
-        @pl.when(c == 1)
+        @pl.when(c == S)
         def _():
             for i in range(2):
                 rdma(
@@ -377,18 +399,14 @@
         rdma(comb, rel, tail_send.at[i], rel_sem.at[0], right).wait_send()
     tail_copy.wait_send()
 
-    @pl.when(c == 0)
+    @pl.when(c == W)
     def _():
         rdma(ubuf, u0, u0_sem.at[0], u0_sem.at[1], partner).wait_send()
-        rdma(wt.at[0, 0:3], wt.at[0, 0:3], xs_sem, zsem.at[0, 0], partner).wait_send()
-        half = nz // 2
-        rdma(wt.at[0:half], wt.at[0:half], rs_sem, zsem.at[0, 0], partner).wait_send()
-        rdma(
-            wt.at[0 : half - 1], wt.at[0 : half - 1], ls_sem, zsem.at[0, 0], partner
-        ).wait_send()
+        for sem, ref in enumerate((wt.at[0:15, 0], wt.at[0:8], wt.at[0:4])):
+            rdma(ref, ref, ws_sem.at[sem], zsem.at[0, 0], partner).wait_send()
         rdma(wt, wt, fs_sem, fsem.at[0], partner).wait_send()
 
-    @pl.when(c == 1)
+    @pl.when(c == S)
     def _():
         rdma(wblk, wt.at[0, 0, 0:16], wd_sem.at[0], wd_sem.at[1], partner).wait_send()
         rdma(pbuf.at[0:3], prec.at[0:3], p_sem.at[0], p_sem.at[1], partner).wait_send()
@@ -406,7 +424,6 @@
         queries, keys, values, gate_code, gate_up, gate_bias, gla_gain,
         conv_input, conv_gate, conv_taps, out_gla, out_conv,
     ):
-        weights = jnp.concatenate([out_gla.T, out_conv.T], axis=1)
         width = HEADS * HV
         vm, dma = pltpu.VMEM, pltpu.SemaphoreType.DMA
         quarter = ROWS // nt
@@ -427,26 +444,28 @@
             vm((16, width), BF16),
             vm((8 + ROWS, width), F32),
             vm((ROWS, 2 * width), BF16),
+            vm((16, 2 * width), BF16),
+            vm((NX, KW, KW), BF16),
             vm((NCHUNK, nt, quarter, CW), BF16),
             vm((NCHUNK, quarter, CW), BF16),
             vm((NCHUNK, quarter, CW), BF16),
             vm((NCHUNK, quarter, CW), BF16),
             vm((NCHUNK, quarter, CW), BF16),
-            dma((nz, NX)), dma((nz,)), dma, dma, dma, dma, dma((2,)),
+            dma((nz, NX)), dma((nz,)), dma((3,)), dma, dma((2,)),
             dma((2,)), dma((5,)), dma((6,)), dma((3,)), dma((5,)), dma((2,)), dma((2,)),
             dma((NCHUNK,)), dma((NCHUNK,)), dma((NCHUNK,)), dma((3,)),
         ]
         return pl.pallas_call(
             functools.partial(layer_kernel, nz, nt),
             out_shape=jax.ShapeDtypeStruct((quarter, 2048), BF16),
-            in_specs=[pl.BlockSpec(memory_space=pltpu.VMEM)] * 11,
+            in_specs=[pl.BlockSpec(memory_space=pltpu.VMEM)] * 12,
             out_specs=pl.BlockSpec(memory_space=pltpu.VMEM),
             scratch_shapes=scratch,
             compiler_params=pltpu.CompilerParams(collective_id=0, has_side_effects=True),
             name="layer",
         )(
-            queries, keys, values, gate_code, gate_up, gate_bias[None], gla_gain[None],
-            conv_input, conv_gate, conv_taps, weights,
+            queries, keys, values, gate_code.T, gate_up, gate_bias[None], gla_gain[None],
+            conv_input, conv_gate, conv_taps, out_gla.T, out_conv.T,
         )
 
     return jax.shard_map(

time: 69.2 us -> 60.1 us (0.87)
  Pallas kernels: 65.1 us -> 58.2 us
  other arithmetic: 1.35 us -> 0 us
  local copies, waits for them, and re-layouts: 2.41 us -> 1.67 us
    pallas_call x1, Pallas kernels: 65.1 us -> 58.2 us  [step(): pl.pallas_call(functools.partial(layer_kernel, nz, nt), out_shape=jax.Sha...]
    concatenate x1 -> x0, other arithmetic: 1.35 us -> none  [step(): weights = jnp.concatenate([out_gla.T, out_conv.T], axis=1)]
    unnamed x4 -> x1, local copies, waits for them, and re-layouts: 2.41 us -> 1.67 us
where the time goes in v2:
time: 60.1 us; the launch traced here: 59.9 us
  Pallas kernels  58.2 us (97%)
  local copies, waits for them, and re-layouts  1.67 us (3%)
    pallas_call x1, Pallas kernels, step(): pl.pallas_call(functools.partial(layer_kernel, nz, nt), out_shape=jax.Sha...  58.2 us
    unnamed x1, local copies, waits for them, and re-layouts  1.67 us

profile of v2, /device:TPU:1, one launch (start us, length us, event | category | flops | bytes accessed | tf_op | source)
XLA Modules:
  0.0 59.9 jit_solution(2628180484910280555)
XLA Ops:
  0.0 58.2 %layer.1 = bf16[64,2048]{1,0:T(8,128)(2,1)} custom-call(bf16[256,256]{1,0:T(8,128)(2,1)} %q.1, bf16[256,256]{1,0:T(8,128)(2,1)} %k.1, bf16[256,512]{1,0:T(8,128)(2,1)} %v.1, bf16[32,256]{1,0:T(8,128)(2,1)} %bitcast.5, bf16[32,256]{1,0:T(8,128)(2,1)} %up.1, f32[1,256]{1,0:T(1,128)} %bitcast.8, f32[1,256]{1,0:T(1,128)} %bitcast.9, bf16[256,512]{1,0:T(8,128)(2,1)} %cin.1, ...), custom_call_target="tpu_custom_call" | custom-call | tf_op jit(solution)/shard_map/layer/pallas_call | solution.py:458
  58.2 1.7 %copy.14 = bf16[64,2048]{1,0:T(8,128)(2,1)} copy(bf16[64,2048]{1,0:T(8,128)(2,1)} %layer.1) | data formatting | bytes 524288

commit v3 on v2

--- a/solution.py
+++ b/solution.py
@@ -18,17 +18,26 @@
 NCHUNK = 8
 CW = 256
 W, S = 1, 0
-ORDER = (0, 1, -1, 2, -2, 3, -3, 4)
 X_ORDER = (1, 3, 2)
-NEAR = (1, 2, 3, 5, 6)
-A_SEND = (1, 2, -1, -2, -3)
-B_SEND = (5, 10)
+NEAR = (1, 2, 3)
+A_SEND = (1, 2, 3, -1, -2)
+B_SEND = (5, -5)
 Z_SENDS = {
     0: (1, -1, 5, -5), 5: (1, -1), -5: (1, -1), -1: (1,), 1: (-1,),
     4: (1,), 6: (-1,), 7: (-1,), -6: (1,), -4: (-1,),
 }
-ARRIVE_ORDER = (1, -1, 5, -5, 2, -2, 4, 6, -4, -6, 3, 7, -3, -7, 8)
-LAG_R, LAG_F = 4, 7
+ARRIVE, RELAY, FINISH = range(3)
+ROW_ORDER = (0, 1, -1, -2, 2, 5, -5, 4, -4, 6, -6, -3, 7, 3, -7, 8)
+BEFORE_STATES = (
+    (ARRIVE, 1), (ARRIVE, -1), (RELAY, 0), (RELAY, 1), (RELAY, -1), (ARRIVE, -2),
+    (ARRIVE, 2), (ARRIVE, 5), (FINISH, 0), (ARRIVE, -5), (ARRIVE, 4), (FINISH, 1),
+    (FINISH, -1), (RELAY, -2), (RELAY, 2), (RELAY, 5), (ARRIVE, 6), (ARRIVE, -4),
+    (RELAY, -5), (RELAY, 4), (ARRIVE, -6), (ARRIVE, 7), (FINISH, -2), (FINISH, 2),
+    (RELAY, -4), (FINISH, 5), (ARRIVE, -3), (ARRIVE, 3), (ARRIVE, 8), (FINISH, -5),
+    (FINISH, 4), (RELAY, 6), (ARRIVE, -7), (RELAY, -6), (RELAY, -3), (FINISH, -4),
+    (RELAY, 7), (RELAY, 3), (RELAY, 8), (RELAY, -7),
+)
+DONE = 4
 NT = (((1,), (1,)), ((), ()))
 TN = (((0,), (0,)), ((), ()))
 
@@ -63,13 +72,15 @@
 def layer_kernel(
     nz,
     nt,
-    q, k, v, code, up, bias, gain, cin, cgate, taps, wgla, wconv,
+    q_in, k_in, v_in, code_in, up_in, bias_in, gain_in, cin_in, cgate_in, taps_in,
+    wgla_in, wconv_in,
     out,
+    q, k, v, code, up, bias, gain, cin, cgate, taps,
     wt, states, through, ubuf, u0, pbuf, prec, abuf, arec, wbuf, brec, rbuf, sin,
     ctail, ext, mix, wblk, sout, part, rel, comb, from_left, from_right,
     zsem, fsem, ws_sem, fs_sem, wd_sem,
     u0_sem, p_sem, a_sem, b_sem, r_sem, sin_sem, c_sem,
-    rel_sem, left_sem, right_sem, tail_send,
+    rel_sem, left_sem, right_sem, tail_send, load_sem, wload_sem,
 ):
     s = lax.axis_index("sp")
     t = lax.axis_index("tp")
@@ -125,6 +136,38 @@
             greet(along_z(d))
             greet(along_z(-d))
 
+    loads = {
+        name: pltpu.make_async_copy(src, dst, load_sem.at[i])
+        for i, (name, src, dst) in enumerate((
+            ("code", code_in, code), ("up", up_in, up), ("bias", bias_in, bias),
+            ("k", k_in, k), ("v", v_in, v), ("cin", cin_in, cin),
+            ("cgate", cgate_in, cgate), ("taps", taps_in, taps), ("q", q_in, q),
+            ("gain", gain_in, gain),
+        ))
+    }
+    own_rows, other_rows = slice(16 * W, 16 * W + 16), slice(16 * S, 16 * S + 16)
+    width = HEADS * HV
+
+    def weight_loads(block):
+        return (
+            pltpu.make_async_copy(wgla_in, block.at[:, 0:width], wload_sem.at[0]),
+            pltpu.make_async_copy(wconv_in, block.at[:, width:], wload_sem.at[1]),
+        )
+
+    @pl.when(c == W)
+    def _():
+        for copy in weight_loads(wt.at[z, x, own_rows]):
+            copy.start()
+
+    @pl.when(c == S)
+    def _():
+        for copy in weight_loads(wblk):
+            copy.start()
+
+    for copy in loads.values():
+        copy.start()
+    for name in ("code", "up", "bias", "k", "v"):
+        loads[name].wait()
     score = lax.dot_general(code[...], up[...], TN, preferred_element_type=F32) + bias[...]
     log_decay = (jnp.minimum(score, 0.0) - jnp.log1p(jnp.exp(-jnp.abs(score)))) / 16.0
     row = lax.broadcasted_iota(jnp.int32, (SEG, SEG), 0)
@@ -157,24 +200,25 @@
         ubuf[h * HV : (h + 1) * HV, :] = acc[h].astype(BF16)
     ubuf[HEADS * HV :, :] = decay_rows(thr[:, :KW], thr[:, KW:])
 
-    own_rows, other_rows = slice(16 * W, 16 * W + 16), slice(16 * S, 16 * S + 16)
-    wblk[:, : HEADS * HV] = wgla[...]
-    wblk[:, HEADS * HV :] = wconv[...]
-
     @pl.when(c == W)
     def _():
-        wt[z, x, own_rows, :] = wblk[...]
+        for copy in weight_loads(wt.at[z, x, own_rows]):
+            copy.wait()
         pl.semaphore_wait(barrier, 12)
 
     @pl.when(c == S)
     def _():
-        pl.semaphore_wait(barrier, 18)
+        for copy in weight_loads(wblk):
+            copy.wait()
+        pl.semaphore_wait(barrier, 14)
 
     tail_copy = rdma(
         cin.at[ROWS - 16 : ROWS], ctail, c_sem.at[0], c_sem.at[1], next_in_order(1)
     )
 
     def conv():
+        loads["cgate"].wait()
+        loads["taps"].wait()
         tail_copy.wait_recv()
         ext[8:, :] = cin[...].astype(F32)
         ext[0:8, :] = jnp.where(s == 0, 0.0, ctail[...].astype(F32)[8:16])
@@ -184,6 +228,8 @@
         mix[:, HEADS * HV :] = (cgate[...].astype(F32) * done).astype(BF16)
 
     def read_out(incoming):
+        loads["q"].wait()
+        loads["gain"].wait()
         for h in range(HEADS):
             for n in range(SEGS):
                 decay = through[n, 0:1, h * KW : (h + 1) * KW]
@@ -202,6 +248,56 @@
     def arrived(h):
         return jnp.concatenate([sin[2 * h], sin[2 * h + 1]], axis=0).astype(F32)
 
+    right, left = along_y(1), along_y(-1)
+    opposite, at_right, at_left = (lax.rem(t + d, nt) for d in (2, 1, 3))
+
+    def row_at(d):
+        return lax.rem(z + d + nz, nz)
+
+    def rows_of(o):
+        return [row_at(d) for d in ROW_ORDER[2 * o : 2 * o + 2]]
+
+    def project(o):
+        w = jnp.concatenate([wt[rr].reshape(CW // 2, 2 * width) for rr in rows_of(o)], axis=0)
+        got = lax.dot_general(mix[...], w, NT, preferred_element_type=F32)
+        part[o] = got.astype(BF16).reshape(nt, ROWS // nt, CW)
+        rdma(
+            part.at[o, opposite], rel.at[o], tail_send.at[0], rel_sem.at[o],
+            right if o % 2 == 0 else left,
+        ).start()
+
+    def send_direct(o):
+        if o % 2 == 0:
+            rdma(
+                part.at[o, at_left], from_right.at[o], tail_send.at[1],
+                right_sem.at[o], left,
+            ).start()
+        else:
+            rdma(
+                part.at[o, at_right], from_left.at[o], tail_send.at[1],
+                left_sem.at[o], right,
+            ).start()
+
+    def combine(o):
+        to = right if o % 2 == 0 else left
+        rdma(part.at[o, 0], rel.at[o], tail_send.at[0], rel_sem.at[o], to).wait_recv()
+        mine = part[o, at_right if o % 2 == 0 else at_left]
+        comb[o] = (rel[o].astype(F32) + mine.astype(F32)).astype(BF16)
+        if o % 2 == 0:
+            rdma(comb.at[o], from_left.at[o], tail_send.at[2], left_sem.at[o], right).start()
+        else:
+            rdma(comb.at[o], from_right.at[o], tail_send.at[2], right_sem.at[o], left).start()
+
+    def conclude(o):
+        rdma(comb.at[o], from_left.at[o], tail_send.at[2], left_sem.at[o], right).wait_recv()
+        rdma(comb.at[o], from_right.at[o], tail_send.at[2], right_sem.at[o], left).wait_recv()
+        total = part[o, t].astype(F32) + from_left[o].astype(F32) + from_right[o].astype(F32)
+        for i, rr in enumerate(rows_of(o)):
+            half = CW // 2
+            out[:, pl.ds(pl.multiple_of(rr * half, half), half)] = total[
+                :, i * half : (i + 1) * half
+            ].astype(BF16)
+
     def send_block(rr, xx, sem, dev):
         block = wt.at[rr, xx]
         rdma(block, block, ws_sem.at[sem], zsem.at[rr, xx], dev).start()
@@ -209,9 +305,6 @@
     def wait_block(rr, xx):
         block = wt.at[rr, xx]
         rdma(block, block, ws_sem.at[0], zsem.at[rr, xx], partner).wait_recv()
-
-    def row_at(d):
-        return lax.rem(z + d + nz, nz)
 
     def x_at(d):
         return lax.rem(x + d, NX)
@@ -239,24 +332,30 @@
     @pl.when(c == W)
     def _():
         rdma(ubuf, u0, u0_sem.at[0], u0_sem.at[1], partner).start()
+        loads["cin"].wait()
         tail_copy.start()
         rdma(wblk, wt.at[z, x, other_rows], wd_sem.at[0], wd_sem.at[1], partner).wait_recv()
         arrive(0)
         conv()
-        order = (0,) + ARRIVE_ORDER
-        for i in range(1, nz + LAG_F):
-            if i < nz:
-                arrive(order[i])
-            if 0 <= i - LAG_R < nz:
-                relay(order[i - LAG_R])
-            if 0 <= i - LAG_F < nz:
-                finish(order[i - LAG_F])
+        for what, d in BEFORE_STATES:
+            (arrive, relay, finish)[what](d)
         rdma(sin, sin, sin_sem.at[0], sin_sem.at[1], partner).wait_recv()
         read_out(arrived)
+        for o in range(DONE):
+            project(o)
+        for o in range(DONE):
+            send_direct(o)
+        for o in range(DONE, NCHUNK):
+            for d in ROW_ORDER[max(2 * o, 9) : 2 * o + 2]:
+                finish(d)
+            project(o)
+        for o in range(DONE, NCHUNK):
+            send_direct(o)
 
     @pl.when(c == S)
     def _():
         rdma(wblk, wt.at[z, x, other_rows], wd_sem.at[0], wd_sem.at[1], partner).start()
+        loads["cin"].wait()
         tail_copy.start()
         rdma(ubuf, u0, u0_sem.at[0], u0_sem.at[1], partner).wait_recv()
 
@@ -301,24 +400,25 @@
         conv()
         for j, d in enumerate(A_SEND):
             rdma(abuf, arec.at[j], a_sem.at[5], a_sem.at[j], along_z(d)).wait_recv()
-        back1, back2, ahead1, ahead2, ahead3 = (pair_in(arec, j) for j in range(5))
-        inner = z <= nz - 4
-        window = only_if(inner & (z >= 2), back2)
-        window = chain(window, only_if(inner & (z >= 1), back1))
+        back1, back2, back3, ahead1, ahead2 = (pair_in(arec, j) for j in range(5))
+        inner = z <= nz - 6
+        window = chain(
+            only_if(inner & (z >= 2), back2), only_if(inner & (z >= 1), back1)
+        )
         window = chain(window, only_if(inner, plane))
         window = chain(window, only_if(inner | (z == nz - 1), ahead1))
         window = chain(window, only_if(inner | (z >= nz - 2), ahead2))
-        wbuf[0:KW, :] = window[1].astype(BF16)
-        wbuf[KW:, :] = decay_rows(window[0])
+        wider = chain(only_if(inner & (z >= 3), back3), window)
+        for j, (decay, state) in enumerate((wider, window)):
+            wbuf[j, 0:KW, :] = state.astype(BF16)
+            wbuf[j, KW:, :] = decay_rows(decay)
         for j, d in enumerate(B_SEND):
-            rdma(wbuf, brec.at[j], b_sem.at[2], b_sem.at[j], along_z(d)).start()
-        oldest = only_if(z >= nz - 1, ahead1)
-        oldest = chain(oldest, only_if(z >= nz - 2, ahead2))
-        oldest = chain(oldest, only_if(z >= nz - 3, ahead3))
+            rdma(wbuf.at[j], brec.at[j], b_sem.at[2], b_sem.at[j], along_z(d)).start()
+        oldest = chain(only_if(z >= nz - 1, ahead1), only_if(z >= nz - 2, ahead2))
         newest = chain(only_if(z >= 2, back2), only_if(z >= 1, back1))
         for j, d in enumerate(B_SEND):
-            rdma(wbuf, brec.at[j], b_sem.at[2], b_sem.at[j], along_z(d)).wait_recv()
-        before = chain(oldest, only_if(z >= 8, pair_in(brec, 1)))
+            rdma(wbuf.at[j], brec.at[j], b_sem.at[2], b_sem.at[j], along_z(d)).wait_recv()
+        before = chain(oldest, only_if(z >= 9, pair_in(brec, 1)))
         before = chain(before, only_if(z >= 3, pair_in(brec, 0)))
         before = chain(before, newest)
         run = before[1]
@@ -349,52 +449,17 @@
                 sout[2 * h : 2 * h + 2] = after_first(h).astype(BF16).reshape(2, KW, KW)
             rdma(sout, sin, sin_sem.at[0], sin_sem.at[1], partner).start()
         read_out(after_first if S == 1 else arrived)
-
-    right, left = along_y(1), along_y(-1)
-    opposite, at_right, at_left = (lax.rem(t + d, nt) for d in (2, 1, 3))
-    zc = z // 2
-    columns = [lax.rem(zc + d + NCHUNK, NCHUNK) for d in ORDER]
-    for o, j in enumerate(columns):
-        @pl.when(c == S)
-        def _():
-            for i in range(2):
-                rdma(
-                    wt.at[2 * j + i], wt.at[2 * j + i], fs_sem, fsem.at[2 * j + i], partner
-                ).wait_recv()
-
-        w = wt[pl.ds(2 * j, 2)].reshape(CW, 2 * HEADS * HV)
-        got = lax.dot_general(mix[...], w, NT, preferred_element_type=F32)
-        part[o] = got.astype(BF16).reshape(nt, ROWS // nt, CW)
-        rdma(
-            part.at[o, opposite], rel.at[o], tail_send.at[0], rel_sem.at[o],
-            right if o % 2 == 0 else left,
-        ).start()
+        for o in range(NCHUNK):
+            for rr in rows_of(o):
+                rdma(wt.at[rr], wt.at[rr], fs_sem, fsem.at[rr], partner).wait_recv()
+            project(o)
+        for o in range(NCHUNK):
+            send_direct(o)
+
     for o in range(NCHUNK):
-        if o % 2 == 0:
-            rdma(
-                part.at[o, at_left], from_right.at[o], tail_send.at[1],
-                right_sem.at[o], left,
-            ).start()
-        else:
-            rdma(
-                part.at[o, at_right], from_left.at[o], tail_send.at[1],
-                left_sem.at[o], right,
-            ).start()
+        combine(o)
     for o in range(NCHUNK):
-        to = right if o % 2 == 0 else left
-        rdma(part.at[o, 0], rel.at[o], tail_send.at[0], rel_sem.at[o], to).wait_recv()
-        mine = part[o, at_right if o % 2 == 0 else at_left]
-        comb[o] = (rel[o].astype(F32) + mine.astype(F32)).astype(BF16)
-        if o % 2 == 0:
-            rdma(comb.at[o], from_left.at[o], tail_send.at[2], left_sem.at[o], right).start()
-        else:
-            rdma(comb.at[o], from_right.at[o], tail_send.at[2], right_sem.at[o], left).start()
-    for o, j in enumerate(columns):
-        rdma(comb.at[o], from_left.at[o], tail_send.at[2], left_sem.at[o], right).wait_recv()
-        rdma(comb.at[o], from_right.at[o], tail_send.at[2], right_sem.at[o], left).wait_recv()
-        total = part[o, t].astype(F32) + from_left[o].astype(F32) + from_right[o].astype(F32)
-        out[:, pl.ds(pl.multiple_of(j * CW, CW), CW)] = total.astype(BF16)
-
+        conclude(o)
     for i in range(3):
         rdma(comb, rel, tail_send.at[i], rel_sem.at[0], right).wait_send()
     tail_copy.wait_send()
@@ -428,6 +493,16 @@
         vm, dma = pltpu.VMEM, pltpu.SemaphoreType.DMA
         quarter = ROWS // nt
         scratch = [
+            vm((ROWS, HEADS * KW), BF16),
+            vm((ROWS, HEADS * KW), BF16),
+            vm((ROWS, width), BF16),
+            vm((32, ROWS), BF16),
+            vm((32, HEADS * KW), BF16),
+            vm((1, HEADS * KW), F32),
+            vm((1, HV), F32),
+            vm((ROWS, width), BF16),
+            vm((ROWS, width), BF16),
+            vm((3, width), F32),
             vm((nz, NX, 32, 2 * width), BF16),
             vm((SEGS, width, KW), F32),
             vm((SEGS, 8, HEADS * KW), F32),
@@ -437,7 +512,7 @@
             vm((NX, KW + 16, KW), BF16),
             vm((KW + 16, KW), BF16),
             vm((5, KW + 16, KW), BF16),
-            vm((KW + 16, KW), BF16),
+            vm((2, KW + 16, KW), BF16),
             vm((2, KW + 16, KW), BF16),
             vm((NX, KW, KW), BF16),
             vm((NX, KW, KW), BF16),
@@ -453,12 +528,12 @@
             vm((NCHUNK, quarter, CW), BF16),
             dma((nz, NX)), dma((nz,)), dma((3,)), dma, dma((2,)),
             dma((2,)), dma((5,)), dma((6,)), dma((3,)), dma((5,)), dma((2,)), dma((2,)),
-            dma((NCHUNK,)), dma((NCHUNK,)), dma((NCHUNK,)), dma((3,)),
+            dma((NCHUNK,)), dma((NCHUNK,)), dma((NCHUNK,)), dma((3,)), dma((10,)), dma((2,)),
         ]
         return pl.pallas_call(
             functools.partial(layer_kernel, nz, nt),
             out_shape=jax.ShapeDtypeStruct((quarter, 2048), BF16),
-            in_specs=[pl.BlockSpec(memory_space=pltpu.VMEM)] * 12,
+            in_specs=[pl.BlockSpec(memory_space=pl.ANY)] * 12,
             out_specs=pl.BlockSpec(memory_space=pltpu.VMEM),
             scratch_shapes=scratch,
             compiler_params=pltpu.CompilerParams(collective_id=0, has_side_effects=True),

time: 60.1 us -> 54.7 us (0.910); the launches traced: 59.9 us -> 53.6 us
  Pallas kernels: 58.2 us -> 52 us
    pallas_call x1, Pallas kernels: 58.2 us -> 52 us  [step(): pl.pallas_call(functools.partial(layer_kernel, nz, nt), out_shape=jax.Sha...]
where the time goes in v3:
time: 54.7 us; the launch traced here: 53.6 us
  Pallas kernels  52 us (95%)
  local copies, waits for them, and re-layouts  1.67 us (3%)
    pallas_call x1, Pallas kernels, step(): pl.pallas_call(functools.partial(layer_kernel, nz, nt), out_shape=jax.Sha...  52 us
    unnamed x1, local copies, waits for them, and re-layouts  1.67 us

profile of v3, /device:TPU:1, one launch (start us, length us, event | category | flops | bytes accessed | tf_op | source)
XLA Modules:
  0.0 53.6 jit_solution(15193291946833177174)
XLA Ops:
  0.0 52.0 %layer.1 = bf16[64,2048]{1,0:T(8,128)(2,1)} custom-call(bf16[256,256]{1,0:T(8,128)(2,1)} %q_in.1, bf16[256,256]{1,0:T(8,128)(2,1)} %k_in.1, bf16[256,512]{1,0:T(8,128)(2,1)} %v_in.1, bf16[32,256]{1,0:T(8,128)(2,1)} %bitcast.5, bf16[32,256]{1,0:T(8,128)(2,1)} %up_in.1, f32[1,256]{1,0:T(1,128)} %bitcast.8, f32[1,256]{1,0:T(1,128)} %bitcast.9, ...), custom_call_target="tpu_custom_call" | custom-call | tf_op jit(solution)/shard_map/layer/pallas_call | solution.py:533
  52.0 1.7 %copy.14 = bf16[64,2048]{1,0:T(8,128)(2,1)} copy(bf16[64,2048]{1,0:T(8,128)(2,1)} %layer.1) | data formatting | bytes 524288

commit v4 on v3

--- a/solution.py
+++ b/solution.py
@@ -20,24 +20,27 @@
 W, S = 1, 0
 X_ORDER = (1, 3, 2)
 NEAR = (1, 2, 3)
-A_SEND = (1, 2, 3, -1, -2)
+W_GREETINGS, S_GREETINGS = 12, 14
+A_SEND = (3, -2, 2, -1, 1)
 B_SEND = (5, -5)
 Z_SENDS = {
-    0: (1, -1, 5, -5), 5: (1, -1), -5: (1, -1), -1: (1,), 1: (-1,),
-    4: (1,), 6: (-1,), 7: (-1,), -6: (1,), -4: (-1,),
+    0: (1, -1, 4, -4), 1: (-1,), -1: (1,), 4: (1, -1), -4: (1, -1),
+    5: (-1,), -5: (1,), 6: (-1,), -6: (1,), 7: (-1,),
 }
-ARRIVE, RELAY, FINISH = range(3)
-ROW_ORDER = (0, 1, -1, -2, 2, 5, -5, 4, -4, 6, -6, -3, 7, 3, -7, 8)
+ARRIVE, RELAY, FINISH, CONV = range(4)
+ROW_ORDER = (0, -1, 1, 4, -2, -4, 2, 5, -5, -6, 6, -3, 3, 7, 8, -7)
 BEFORE_STATES = (
-    (ARRIVE, 1), (ARRIVE, -1), (RELAY, 0), (RELAY, 1), (RELAY, -1), (ARRIVE, -2),
-    (ARRIVE, 2), (ARRIVE, 5), (FINISH, 0), (ARRIVE, -5), (ARRIVE, 4), (FINISH, 1),
-    (FINISH, -1), (RELAY, -2), (RELAY, 2), (RELAY, 5), (ARRIVE, 6), (ARRIVE, -4),
-    (RELAY, -5), (RELAY, 4), (ARRIVE, -6), (ARRIVE, 7), (FINISH, -2), (FINISH, 2),
-    (RELAY, -4), (FINISH, 5), (ARRIVE, -3), (ARRIVE, 3), (ARRIVE, 8), (FINISH, -5),
-    (FINISH, 4), (RELAY, 6), (ARRIVE, -7), (RELAY, -6), (RELAY, -3), (FINISH, -4),
-    (RELAY, 7), (RELAY, 3), (RELAY, 8), (RELAY, -7),
+    (ARRIVE, 1), (ARRIVE, -1), (RELAY, 0), (ARRIVE, 4), (RELAY, 1), (RELAY, -1),
+    (CONV, 0), (ARRIVE, -2), (ARRIVE, 2), (ARRIVE, -4), (RELAY, 4), (FINISH, 0),
+    (ARRIVE, 5), (ARRIVE, -3), (FINISH, -1), (FINISH, 1), (RELAY, -2), (ARRIVE, -5),
+    (RELAY, -4), (RELAY, 2), (ARRIVE, 6), (RELAY, 5), (FINISH, 4), (ARRIVE, -6),
+    (ARRIVE, 3), (FINISH, -2), (RELAY, -5), (ARRIVE, 7), (ARRIVE, -7), (FINISH, -4),
+    (FINISH, 2), (RELAY, -6), (FINISH, 5), (RELAY, -3), (ARRIVE, 8), (RELAY, 6),
+    (RELAY, 3), (FINISH, -5), (RELAY, 7), (RELAY, -7), (RELAY, 8),
 )
-DONE = 4
+W_COMBINES = ((), (), (), (), (), (), (), tuple(range(8)))
+S_COMBINES = ((), (), (), (0,), (), (1,), (), (2, 3, 4, 5, 6, 7))
+LAST_ROWS = ((-6, 6), (-3, 3), (7,), (8, -7), (), (), (), ())
 NT = (((1,), (1,)), ((), ()))
 TN = (((0,), (0,)), ((), ()))
 
@@ -126,7 +129,7 @@
 
     @pl.when(c == W)
     def _():
-        for d in (1, 5):
+        for d in (1, 4):
             greet(along_z(d))
             greet(along_z(-d))
 
@@ -166,7 +169,14 @@
 
     for copy in loads.values():
         copy.start()
-    for name in ("code", "up", "bias", "k", "v"):
+    @pl.when(c == S)
+    def _():
+        for copy in weight_loads(wblk):
+            copy.wait()
+        pl.semaphore_wait(barrier, S_GREETINGS)
+        rdma(wblk, wt.at[z, x, other_rows], wd_sem.at[0], wd_sem.at[1], partner).start()
+
+    for name in ("code", "up", "bias"):
         loads[name].wait()
     score = lax.dot_general(code[...], up[...], TN, preferred_element_type=F32) + bias[...]
     log_decay = (jnp.minimum(score, 0.0) - jnp.log1p(jnp.exp(-jnp.abs(score)))) / 16.0
@@ -180,6 +190,9 @@
         rest = jnp.dot(
             later, here, preferred_element_type=F32, precision=lax.Precision.HIGHEST
         )
+        if n == 0:
+            loads["k"].wait()
+            loads["v"].wait()
         scaled = (k[n * SEG : (n + 1) * SEG, :].astype(F32) * jnp.exp(rest)).astype(BF16)
         seg_decay = jnp.exp(rest[0:1] + here[0:1])
         thr = seg_decay if n == 0 else thr * seg_decay
@@ -204,13 +217,7 @@
     def _():
         for copy in weight_loads(wt.at[z, x, own_rows]):
             copy.wait()
-        pl.semaphore_wait(barrier, 12)
-
-    @pl.when(c == S)
-    def _():
-        for copy in weight_loads(wblk):
-            copy.wait()
-        pl.semaphore_wait(barrier, 14)
+        pl.semaphore_wait(barrier, W_GREETINGS)
 
     tail_copy = rdma(
         cin.at[ROWS - 16 : ROWS], ctail, c_sem.at[0], c_sem.at[1], next_in_order(1)
@@ -336,25 +343,20 @@
         tail_copy.start()
         rdma(wblk, wt.at[z, x, other_rows], wd_sem.at[0], wd_sem.at[1], partner).wait_recv()
         arrive(0)
-        conv()
         for what, d in BEFORE_STATES:
-            (arrive, relay, finish)[what](d)
+            (arrive, relay, finish, lambda _: conv())[what](d)
         rdma(sin, sin, sin_sem.at[0], sin_sem.at[1], partner).wait_recv()
         read_out(arrived)
-        for o in range(DONE):
+        for o in range(NCHUNK):
             project(o)
-        for o in range(DONE):
+            for d in LAST_ROWS[o]:
+                finish(d)
             send_direct(o)
-        for o in range(DONE, NCHUNK):
-            for d in ROW_ORDER[max(2 * o, 9) : 2 * o + 2]:
-                finish(d)
-            project(o)
-        for o in range(DONE, NCHUNK):
-            send_direct(o)
+            for i in W_COMBINES[o]:
+                combine(i)
 
     @pl.when(c == S)
     def _():
-        rdma(wblk, wt.at[z, x, other_rows], wd_sem.at[0], wd_sem.at[1], partner).start()
         loads["cin"].wait()
         tail_copy.start()
         rdma(ubuf, u0, u0_sem.at[0], u0_sem.at[1], partner).wait_recv()
@@ -374,7 +376,7 @@
             both = chain(first(*part_of), second(*part_of))
             pbuf[i, 0:KW, :] = both[1].astype(BF16)
             pbuf[i, KW:, :] = decay_rows(both[0])
-        for j, d in enumerate((1, 3, 2)):
+        for d in (2, 1, 3):
             rdma(
                 pbuf.at[lax.rem(x + d, NX)], prec.at[x],
                 p_sem.at[0], p_sem.at[1 + d], along_x(d),
@@ -400,7 +402,7 @@
         conv()
         for j, d in enumerate(A_SEND):
             rdma(abuf, arec.at[j], a_sem.at[5], a_sem.at[j], along_z(d)).wait_recv()
-        back1, back2, back3, ahead1, ahead2 = (pair_in(arec, j) for j in range(5))
+        back3, ahead2, back2, ahead1, back1 = (pair_in(arec, j) for j in range(5))
         inner = z <= nz - 6
         window = chain(
             only_if(inner & (z >= 2), back2), only_if(inner & (z >= 1), back1)
@@ -426,7 +428,7 @@
             rbuf[i] = run.astype(BF16)
             if i < NX - 1:
                 run = chips[i][0] * run + chips[i][1]
-        for d in (1, 3, 2):
+        for d in (2, 1, 3):
             rdma(
                 rbuf.at[lax.rem(x + d, NX)], sin.at[x],
                 r_sem.at[0], r_sem.at[1 + d], along_x(d),
@@ -453,11 +455,10 @@
             for rr in rows_of(o):
                 rdma(wt.at[rr], wt.at[rr], fs_sem, fsem.at[rr], partner).wait_recv()
             project(o)
-        for o in range(NCHUNK):
             send_direct(o)
-
-    for o in range(NCHUNK):
-        combine(o)
+            for i in S_COMBINES[o]:
+                combine(i)
+
     for o in range(NCHUNK):
         conclude(o)
     for i in range(3):
@@ -532,7 +533,7 @@
         ]
         return pl.pallas_call(
             functools.partial(layer_kernel, nz, nt),
-            out_shape=jax.ShapeDtypeStruct((quarter, 2048), BF16),
+            out_shape=pltpu.VMEM((quarter, 2048), BF16),
             in_specs=[pl.BlockSpec(memory_space=pl.ANY)] * 12,
             out_specs=pl.BlockSpec(memory_space=pltpu.VMEM),
             scratch_shapes=scratch,

time: 54.7 us -> 51.6 us (0.943); the launches traced: 53.6 us -> 51.4 us
  Pallas kernels: 52 us -> 50.7 us
  local copies, waits for them, and re-layouts: 1.67 us -> 0.71 us
    pallas_call x1, Pallas kernels: 52 us -> 50.7 us  [step(): pl.pallas_call(functools.partial(layer_kernel, nz, nt), out_shape=pltpu.V...]
    unnamed x1, local copies, waits for them, and re-layouts: 1.67 us -> 0.71 us
where the time goes in v4:
time: 51.6 us; the launch traced here: 51.4 us
  Pallas kernels  50.7 us (98%)
  local copies, waits for them, and re-layouts  0.71 us (1%)
    pallas_call x1, Pallas kernels, step(): pl.pallas_call(functools.partial(layer_kernel, nz, nt), out_shape=pltpu.V...  50.7 us

profile of v4, /device:TPU:1, one launch (start us, length us, event | category | flops | bytes accessed | tf_op | source)
XLA Modules:
  0.0 51.4 jit_solution(16112860422784352539)
XLA Ops:
  0.0 50.7 %layer.1 = bf16[64,2048]{1,0:T(8,128)(2,1)S(1)} custom-call(bf16[256,256]{1,0:T(8,128)(2,1)} %q_in.1, bf16[256,256]{1,0:T(8,128)(2,1)} %k_in.1, bf16[256,512]{1,0:T(8,128)(2,1)} %v_in.1, bf16[32,256]{1,0:T(8,128)(2,1)} %bitcast.5, bf16[32,256]{1,0:T(8,128)(2,1)} %up_in.1, f32[1,256]{1,0:T(1,128)} %bitcast.8, f32[1,256]{1,0:T(1,128)} %bitcast.9, ...), custom_call_target="tpu_custom_call" | custom-call | tf_op jit(solution)/shard_map/layer/pallas_call | solution.py:534
  50.7 0.7 %copy.14 = bf16[64,2048]{1,0:T(8,128)(2,1)} copy(bf16[64,2048]{1,0:T(8,128)(2,1)S(1)} %layer.1) | data formatting | bytes 524288

commit v5 on v4

--- a/solution.py
+++ b/solution.py
@@ -169,13 +169,6 @@
 
     for copy in loads.values():
         copy.start()
-    @pl.when(c == S)
-    def _():
-        for copy in weight_loads(wblk):
-            copy.wait()
-        pl.semaphore_wait(barrier, S_GREETINGS)
-        rdma(wblk, wt.at[z, x, other_rows], wd_sem.at[0], wd_sem.at[1], partner).start()
-
     for name in ("code", "up", "bias"):
         loads[name].wait()
     score = lax.dot_general(code[...], up[...], TN, preferred_element_type=F32) + bias[...]
@@ -183,18 +176,29 @@
     row = lax.broadcasted_iota(jnp.int32, (SEG, SEG), 0)
     col = lax.broadcasted_iota(jnp.int32, (SEG, SEG), 1)
     later = (col > row).astype(F32)
-    acc = [None] * HEADS
-    thr = None
+    to_end, seg_decays = [], []
     for n in range(SEGS):
         here = log_decay[n * SEG : (n + 1) * SEG]
         rest = jnp.dot(
             later, here, preferred_element_type=F32, precision=lax.Precision.HIGHEST
         )
-        if n == 0:
-            loads["k"].wait()
-            loads["v"].wait()
-        scaled = (k[n * SEG : (n + 1) * SEG, :].astype(F32) * jnp.exp(rest)).astype(BF16)
-        seg_decay = jnp.exp(rest[0:1] + here[0:1])
+        to_end.append(jnp.exp(rest))
+        seg_decays.append(jnp.exp(rest[0:1] + here[0:1]))
+
+    @pl.when(c == S)
+    def _():
+        for copy in weight_loads(wblk):
+            copy.wait()
+        pl.semaphore_wait(barrier, S_GREETINGS)
+        rdma(wblk, wt.at[z, x, other_rows], wd_sem.at[0], wd_sem.at[1], partner).start()
+
+    loads["k"].wait()
+    loads["v"].wait()
+    acc = [None] * HEADS
+    thr = None
+    for n in range(SEGS):
+        seg_decay = seg_decays[n]
+        scaled = (k[n * SEG : (n + 1) * SEG, :].astype(F32) * to_end[n]).astype(BF16)
         thr = seg_decay if n == 0 else thr * seg_decay
         through[n] = jnp.broadcast_to(thr, (8, HEADS * KW))
         for h in range(HEADS):

time: 51.6 us -> 51.3 us (level)
  no operation moved by 1% of the time
where the time goes in v5:
time: 51.3 us; the launch traced here: 51.1 us
  Pallas kernels  50.4 us (98%)
  local copies, waits for them, and re-layouts  0.71 us (1%)
    pallas_call x1, Pallas kernels, step(): pl.pallas_call(functools.partial(layer_kernel, nz, nt), out_shape=pltpu.V...  50.4 us

profile of v5, /device:TPU:1, one launch (start us, length us, event | category | flops | bytes accessed | tf_op | source)
XLA Modules:
  0.0 51.1 jit_solution(4717609886810365027)
XLA Ops:
  0.0 50.4 %layer.1 = bf16[64,2048]{1,0:T(8,128)(2,1)S(1)} custom-call(bf16[256,256]{1,0:T(8,128)(2,1)} %q_in.1, bf16[256,256]{1,0:T(8,128)(2,1)} %k_in.1, bf16[256,512]{1,0:T(8,128)(2,1)} %v_in.1, bf16[32,256]{1,0:T(8,128)(2,1)} %bitcast.5, bf16[32,256]{1,0:T(8,128)(2,1)} %up_in.1, f32[1,256]{1,0:T(1,128)} %bitcast.8, f32[1,256]{1,0:T(1,128)} %bitcast.9, ...), custom_call_target="tpu_custom_call" | custom-call | tf_op jit(solution)/shard_map/layer/pallas_call | solution.py:538
  50.4 0.7 %copy.14 = bf16[64,2048]{1,0:T(8,128)(2,1)} copy(bf16[64,2048]{1,0:T(8,128)(2,1)S(1)} %layer.1) | data formatting | bytes 524288

commit v6 on v5

--- a/solution.py
+++ b/solution.py
@@ -36,11 +36,11 @@
     (RELAY, -4), (RELAY, 2), (ARRIVE, 6), (RELAY, 5), (FINISH, 4), (ARRIVE, -6),
     (ARRIVE, 3), (FINISH, -2), (RELAY, -5), (ARRIVE, 7), (ARRIVE, -7), (FINISH, -4),
     (FINISH, 2), (RELAY, -6), (FINISH, 5), (RELAY, -3), (ARRIVE, 8), (RELAY, 6),
-    (RELAY, 3), (FINISH, -5), (RELAY, 7), (RELAY, -7), (RELAY, 8),
+    (RELAY, 3), (FINISH, -5), (RELAY, 7), (RELAY, -7), (RELAY, 8), (FINISH, -6), (FINISH, 6),
 )
 W_COMBINES = ((), (), (), (), (), (), (), tuple(range(8)))
 S_COMBINES = ((), (), (), (0,), (), (1,), (), (2, 3, 4, 5, 6, 7))
-LAST_ROWS = ((-6, 6), (-3, 3), (7,), (8, -7), (), (), (), ())
+LAST_ROWS = ((-3,), (3, 7), (8,), (-7,), (), (), (), ())
 NT = (((1,), (1,)), ((), ()))
 TN = (((0,), (0,)), ((), ()))
 

time: 51.3 us -> 51.5 us (level)
  no operation moved by 1% of the time
where the time goes in v6:
time: 51.5 us; the launch traced here: 51.4 us
  Pallas kernels  50.6 us (98%)
  local copies, waits for them, and re-layouts  0.71 us (1%)
    pallas_call x1, Pallas kernels, step(): pl.pallas_call(functools.partial(layer_kernel, nz, nt), out_shape=pltpu.V...  50.6 us

profile of v6, /device:TPU:1, one launch (start us, length us, event | category | flops | bytes accessed | tf_op | source)
XLA Modules:
  0.0 51.4 jit_solution(7710469801530550256)
XLA Ops:
  0.0 50.6 %layer.1 = bf16[64,2048]{1,0:T(8,128)(2,1)S(1)} custom-call(bf16[256,256]{1,0:T(8,128)(2,1)} %q_in.1, bf16[256,256]{1,0:T(8,128)(2,1)} %k_in.1, bf16[256,512]{1,0:T(8,128)(2,1)} %v_in.1, bf16[32,256]{1,0:T(8,128)(2,1)} %bitcast.5, bf16[32,256]{1,0:T(8,128)(2,1)} %up_in.1, f32[1,256]{1,0:T(1,128)} %bitcast.8, f32[1,256]{1,0:T(1,128)} %bitcast.9, ...), custom_call_target="tpu_custom_call" | custom-call | tf_op jit(solution)/shard_map/layer/pallas_call | solution.py:538
  50.6 0.7 %copy.14 = bf16[64,2048]{1,0:T(8,128)(2,1)} copy(bf16[64,2048]{1,0:T(8,128)(2,1)S(1)} %layer.1) | data formatting | bytes 524288
